TPU v7x, 32 devices: a whole 2x2x4 slice. The times are simulated.
32 devices in a mesh: sp: 4 (over y, x), tp: 8 (over z, core).
Axes of the slice: x: 2, y: 2, z: 4, core: 2. Of those that a mesh axis runs over, the one named last changes fastest.
Arguments:
- tokens: bfloat16 [2048, 4096], P('sp', 'tp'), may hold values from -6 to 6
- pre_gain: float32 [2, 4096], replicated, may hold values from 0.1 to 1.9
- w_value: bfloat16 [2, 4096, 4096], P(None, 'sp', 'tp'), may hold values from -0.09375 to 0.09375
- w_gate: bfloat16 [2, 4096, 4096], P(None, 'sp', 'tp'), may hold values from -0.09375 to 0.09375
- conv_taps: float32 [2, 31, 4096], P(None, None, 'tp'), may hold values from -3.5 to 3.5
- conv_bias: float32 [2, 4096], P(None, 'tp'), may hold values from -3 to 3
- norm_gain: float32 [2, 4096], P(None, 'tp'), may hold values from 0.1 to 1.9
- norm_bias: float32 [2, 4096], P(None, 'tp'), may hold values from -3 to 3
- w_out: bfloat16 [2, 4096, 4096], P(None, 'sp', 'tp'), may hold values from -0.09375 to 0.09375
- post_gain: float32 [2, 4096], P(None, 'tp'), may hold values from 0.1 to 1.9
Outputs:
- stream: bfloat16 [2048, 4096], P('sp', 'tp')
All inputs are finite; a program needn't handle non-finite values.
Results may differ from a plain program's by a relative error of at most 0.009.
Values may be sent and summed in bfloat16 or wider, within the bound.
A program may use at most 64 MiB of HBM per device.

v0:
```python
import functools

import jax
import jax.numpy as jnp
from jax import lax
from jax.experimental import pallas as pl
from jax.experimental.pallas import tpu as pltpu
from jax.sharding import PartitionSpec as P

MESH = pl.DeviceIdType.MESH
LANES = 128
HALVES = 2
AHEAD = 2
ROW_TILE = 64
HALO_ROWS = 32


def gray_of(position, count):
    bits = [(position // 2**k) % 2 for k in range(count.bit_length())]
    return sum(((bits[k] + bits[k + 1]) % 2) * 2**k for k in range(count.bit_length() - 1))


def position_of(index, count):
    bits = [(index // 2**k) % 2 for k in range(count.bit_length() - 1)]
    return sum((sum(bits[k:]) % 2) * 2**k for k in range(count.bit_length() - 1))


def loop(count, body):
    def step(index, carry):
        body(index)
        return carry

    lax.fori_loop(0, count, step, 0)


def remote(src, dst, send_sem, recv_sem, axis, target):
    return pltpu.make_async_remote_copy(
        src_ref=src,
        dst_ref=dst,
        send_sem=send_sem,
        recv_sem=recv_sem,
        device_id={axis: target},
        device_id_type=MESH,
    )


def module_kernel(
    ring,
    count,
    tok_ref,
    pre_ref,
    value_ref,
    gate_ref,
    wout_ref,
    taps_ref,
    bias_ref,
    ngain_ref,
    nbias_ref,
    post_ref,
    out_ref,
    w_all,
    u_all,
    f_all,
    mixed,
    acc,
    padded,
    row_a,
    row_b,
    scale_ref,
    shift_ref,
    stream,
    halo_out,
    halo_in,
    stat_out,
    stat_in,
    params,
    z_up,
    z_down,
    z_recv,
    side_send,
    side_recv,
    ahead_send,
    ahead_recv,
    behind_send,
    behind_recv,
    own_sem,
    stat_send,
    stat_recv,
    par_send,
    par_recv,
    halo_send,
    halo_recv,
):
    layers, depth, width = value_ref.shape
    rows = tok_ref.shape[0]
    model = width * count
    tap_count = taps_ref.shape[1]
    chips = count // 2
    half_rows = rows // HALVES
    strips = width // LANES
    groups = rows // LANES
    half_order = tuple(reversed(range(HALVES)))
    pieces = max(1, min(4, depth // 256))
    piece = depth // pieces
    turns = ring // 2

    me = lax.axis_index("tp")
    z = me // 2
    core = me - 2 * z
    partner = me + 1 - 2 * core
    has_up = z < chips - 1
    has_down = z > 0
    spot = lax.axis_index("sp")
    at = position_of(spot, ring)
    ahead = gray_of((at + 1) % ring, ring)
    behind = gray_of((at + ring - 1) % ring, ring)
    has_next = spot < ring - 1
    has_prev = spot > 0

    barrier = pltpu.get_barrier_semaphore()
    for step in range(1, count):
        pl.semaphore_signal(
            barrier, inc=1, device_id={"tp": lax.rem(me + step, count)}, device_id_type=MESH
        )
    pl.semaphore_signal(barrier, inc=1, device_id={"sp": ahead}, device_id_type=MESH)
    pl.semaphore_signal(barrier, inc=1, device_id={"sp": behind}, device_id_type=MESH)

    @pl.when(has_next)
    def _():
        pl.semaphore_signal(barrier, inc=1, device_id={"sp": spot + 1}, device_id_type=MESH)

    @pl.when(has_prev)
    def _():
        pl.semaphore_signal(barrier, inc=1, device_id={"sp": spot - 1}, device_id_type=MESH)

    pl.semaphore_wait(
        barrier, count + 1 + has_next.astype(jnp.int32) + has_prev.astype(jnp.int32)
    )

    sources = (value_ref, gate_ref, wout_ref)
    chunk_total = 3 * layers * pieces

    def held(chunk, owner, first, size):
        start = owner * depth + (chunk % pieces) * piece + first
        return w_all.at[chunk // pieces, pl.ds(pl.multiple_of(start, size), size), :]

    def ring_copy(chunk, step, sign):
        owner = gray_of((at + ring - sign * step) % ring, ring)
        last = step == turns - 1
        size = piece // 2 if last else piece
        first = piece // 2 if last and sign < 0 else 0
        there = held(chunk, owner, first, size)
        projection = chunk // pieces
        own = sources[projection % 3].at[
            projection // 3, pl.ds((chunk % pieces) * piece + first, size), :
        ]
        sends, recvs, target = (
            (ahead_send, ahead_recv, ahead) if sign > 0 else (behind_send, behind_recv, behind)
        )
        return remote(
            own if step == 0 else there,
            there,
            sends.at[chunk, step],
            recvs.at[chunk, step],
            "sp",
            target,
        )

    def own_copy(chunk):
        projection = chunk // pieces
        return pltpu.make_async_copy(
            sources[projection % 3].at[projection // 3, pl.ds((chunk % pieces) * piece, piece), :],
            held(chunk, spot, 0, piece),
            own_sem.at[chunk],
        )

    def start_chunk(chunk):
        if chunk < chunk_total:
            ring_copy(chunk, 0, 1).start()
            ring_copy(chunk, 0, -1).start()
            own_copy(chunk).start()

    def turn_chunk(chunk):
        for step in range(turns - 1):
            ring_copy(chunk, step, 1).wait_recv()
            ring_copy(chunk, step + 1, 1).start()
            ring_copy(chunk, step, -1).wait_recv()
            ring_copy(chunk, step + 1, -1).start()
        start_chunk(chunk + AHEAD)

    def finish_chunk(chunk):
        ring_copy(chunk, turns - 1, 1).wait_recv()
        ring_copy(chunk, turns - 1, -1).wait_recv()
        own_copy(chunk).wait()

    def stage(q):
        return (u_all if q % 2 == 0 else f_all).at[q // 2]

    def part(q, block, half):
        return stage(q).at[block, pl.ds(half * half_rows, half_rows), :]

    def up(q, chip, half):
        there = part(q, 2 * chip + core, half)
        return remote(
            there, there, z_up.at[q, chip, half], z_recv.at[q, chip, half], "tp", me + 2
        )

    def down(q, chip, half):
        there = part(q, 2 * chip + core, half)
        return remote(
            there, there, z_down.at[q, chip, half], z_recv.at[q, chip, half], "tp", me - 2
        )

    def side(q, chip, half):
        there = part(q, 2 * chip + core, half)
        return remote(
            there, there, side_send.at[q, chip, half], side_recv.at[q, chip, half], "tp", partner
        )

    def side_wait(q, chip, half):
        there = part(q, 2 * chip + 1 - core, half)
        remote(
            there, there, side_send.at[q, chip, half], side_recv.at[q, chip, half], "tp", partner
        ).wait_recv()

    def send_own(q, half):
        @pl.when(has_up)
        def _():
            up(q, z, half).start()

        @pl.when(has_down)
        def _():
            down(q, z, half).start()

        side(q, z, half).start()

    low = z + (2 * z > chips - 1).astype(jnp.int32) * (chips - 1 - 2 * z)
    upward = 1 - 2 * (2 * z > chips - 1).astype(jnp.int32)

    def arrival(index):
        both = (index < 2 * low).astype(jnp.int32)
        paired = z + (index // 2 + 1) * (1 if index % 2 else -1)
        alone = z + (index - low + 1) * upward
        return both * paired + (1 - both) * alone

    def relay(q, index, half):
        chip = arrival(index)
        there = part(q, 2 * chip + core, half)
        remote(
            there, there, z_up.at[q, chip, half], z_recv.at[q, chip, half], "tp", partner
        ).wait_recv()

        @pl.when((chip < z) & has_up)
        def _():
            up(q, chip, half).start()

        @pl.when((chip > z) & has_down)
        def _():
            down(q, chip, half).start()

        side(q, chip, half).start()

    def drain(q):
        def chip_step(chip):
            for half in range(HALVES):
                side(q, chip, half).wait_send()

                @pl.when(has_up & (chip <= z))
                def _():
                    up(q, chip, half).wait_send()

                @pl.when(has_down & (chip >= z))
                def _():
                    down(q, chip, half).wait_send()

        loop(chips, chip_step)

    def stat_copy(event, step):
        return remote(
            stat_out.at[event],
            stat_in.at[event, step - 1],
            stat_send.at[event, step - 1],
            stat_recv.at[event, step - 1],
            "tp",
            lax.rem(me + step, count),
        )

    def pack_rows(event, base, ref):
        for group in range(groups):
            turned = ref[group * LANES : (group + 1) * LANES, :].T
            stat_out[event, base + group : base + group + 1, :] = jnp.sum(
                turned, axis=0, keepdims=True
            )

    def send_stats(event):
        for step in range(1, count):
            stat_copy(event, step).start()

    def total_stats(event):
        total = stat_out[event]
        for step in range(1, count):
            stat_copy(event, step).wait_recv()
            total = total + stat_in[event, step - 1]
        return total

    def spread_rows(ref, packed, base):
        for group in range(groups):
            line = packed[base + group : base + group + 1, :]
            ref[group * LANES : (group + 1) * LANES, :] = jnp.broadcast_to(
                line, (LANES, LANES)
            ).T

    def strip(index):
        return slice(index * LANES, (index + 1) * LANES)

    def tile_at(base, index):
        return pl.ds(pl.multiple_of(base + index * ROW_TILE, ROW_TILE), ROW_TILE)

    half_tiles = half_rows // ROW_TILE

    def emit_u(layer, half, source):
        def body(index):
            at_rows = tile_at(half * half_rows, index)
            values = source(at_rows)
            squares = jnp.zeros((ROW_TILE, LANES), jnp.float32)
            for s in range(strips):
                own = values[:, strip(s)]
                squares = squares + own * own
            row_a[at_rows, :] = squares
            gain = pre_ref[layer : layer + 1, pl.ds(pl.multiple_of(me * width, width), width)]
            u_all[layer, me, at_rows, :] = (values * gain).astype(jnp.bfloat16)

        loop(half_tiles, body)

    column_tile = min(256, width)

    def columns(index):
        return pl.ds(pl.multiple_of(index * column_tile, column_tile), column_tile)

    def project(layer, which, chunk):
        offset = (chunk % pieces) * piece

        def body(index):
            total = None
            for owner in range(ring):
                first = owner * depth + offset
                block, column = first // width, first % width
                product = jnp.dot(
                    u_all[layer, block, :, column : column + piece],
                    w_all[3 * layer + which, first : first + piece, columns(index)],
                    preferred_element_type=jnp.float32,
                )
                total = product if total is None else total + product
            if chunk % pieces == 0:
                acc[which, :, columns(index)] = total
            else:
                acc[which, :, columns(index)] += total

        loop(width // column_tile, body)

    def gated(layer, half):
        def body(index):
            at_rows = tile_at(half * half_rows, index)
            scale = scale_ref[at_rows, :]
            for s in range(strips):
                value = acc[0, at_rows, strip(s)] * scale
                gate = acc[1, at_rows, strip(s)] * scale
                glu = (value * (0.5 * (1.0 + jnp.tanh(0.5 * gate)))).astype(jnp.bfloat16)
                padded[
                    s,
                    pl.ds(
                        pl.multiple_of(HALO_ROWS + half * half_rows + index * ROW_TILE, 8), ROW_TILE
                    ),
                    :,
                ] = glu.astype(jnp.float32)

        loop(half_tiles, body)

    def filter_rows(layer, half):
        def body(index):
            at_rows = tile_at(half * half_rows, index)
            start = half * half_rows + index * ROW_TILE + HALO_ROWS - (tap_count - 1)
            first = jnp.zeros((ROW_TILE, LANES), jnp.float32)
            second = jnp.zeros((ROW_TILE, LANES), jnp.float32)
            for s in range(strips):
                total = jnp.zeros((ROW_TILE, LANES), jnp.float32) + bias_ref[
                    layer : layer + 1, strip(s)
                ]
                for tap in range(tap_count):
                    total = (
                        total
                        + padded[s, pl.ds(start + tap, ROW_TILE), :]
                        * taps_ref[layer, tap : tap + 1, strip(s)]
                    )
                f_all[layer, me, at_rows, strip(s)] = total.astype(jnp.bfloat16)
                first = first + total
                second = second + total * total
            row_a[at_rows, :] = first
            row_b[at_rows, :] = second

        loop(half_tiles, body)

    def mix(layer, chip, half):
        for c in range(2):
            block = 2 * chip + c
            gains = params[block, 2 * layer : 2 * layer + 1, :]
            biases = params[block, 2 * layer + 1 : 2 * layer + 2, :]

            def body(index):
                at_rows = tile_at(half * half_rows, index)
                scale = scale_ref[at_rows, :]
                shift = shift_ref[at_rows, :]
                for s in range(strips):
                    shaped = f_all[layer, block, at_rows, strip(s)].astype(jnp.float32) * scale
                    shaped = (shaped - shift) * gains[:, strip(s)] + biases[:, strip(s)]
                    mixed[block, at_rows, strip(s)] = (
                        shaped * (0.5 * (1.0 + jnp.tanh(0.5 * shaped)))
                    ).astype(jnp.bfloat16)

            loop(half_tiles, body)

    def merge(layer, chip, half, first):
        at_rows = pl.ds(half * half_rows, half_rows)

        def body(index):
            total = None
            for c in range(2):
                block = 2 * chip + c
                product = jnp.dot(
                    mixed[block, at_rows, :],
                    w_all[
                        3 * layer + 2,
                        pl.ds(pl.multiple_of(block * width, width), width),
                        columns(index),
                    ],
                    preferred_element_type=jnp.float32,
                )
                total = product if total is None else total + product
            if first:
                acc[0, at_rows, columns(index)] = total
            else:
                acc[0, at_rows, columns(index)] += total

        loop(width // column_tile, body)

    for chunk in range(AHEAD):
        start_chunk(chunk)

    def from_tokens(at_rows):
        return tok_ref[at_rows, :].astype(jnp.float32)

    for half in half_order:
        emit_u(0, half, from_tokens)
        if half == half_order[0]:
            for layer in range(layers):
                params[me, 2 * layer : 2 * layer + 1, :] = ngain_ref[layer : layer + 1, :]
                params[me, 2 * layer + 1 : 2 * layer + 2, :] = nbias_ref[layer : layer + 1, :]
        send_own(0, half)

    def param_copy(step):
        return remote(
            params.at[me],
            params.at[me],
            par_send.at[step - 1],
            par_recv.at[step - 1],
            "tp",
            lax.rem(me + step, count),
        )

    pack_rows(0, 0, row_a)
    send_stats(0)
    for step in range(1, count):
        param_copy(step).start()

    def halo_copy(layer):
        return remote(
            halo_out.at[layer],
            halo_in.at[layer],
            halo_send.at[layer],
            halo_recv.at[layer],
            "sp",
            lax.rem(spot + 1, ring),
        )

    relays = [(index, half) for index in range(chips - 1) for half in half_order]

    def interleave(q, chunks, after):
        chunks = list(chunks)
        for number, (index, half) in enumerate(relays):
            relay(q, index, half)
            while chunks and len(chunks) * len(relays) > (len(relays) - number - 1) * pieces:
                turn_chunk(chunks.pop(0))
            after(index, half)
        for chunk in chunks:
            turn_chunk(chunk)

    for layer in range(layers):
        base = 3 * layer * pieces
        q = 2 * layer
        event = 3 * layer
        interleave(q, range(base, base + pieces), lambda index, half: None)
        for half in half_order:
            side_wait(q, z, half)
            for index in range(chips - 1):
                side_wait(q, arrival(index), half)
        norm = lax.rsqrt(total_stats(event) / model + 1e-06)
        spread_rows(scale_ref, norm, 0)
        for chunk in range(base, base + pieces):
            finish_chunk(chunk)
            project(layer, 0, chunk)
            turn_chunk(chunk + pieces)
        for chunk in range(base + pieces, base + 2 * pieces):
            finish_chunk(chunk)
            project(layer, 1, chunk)

        for half in half_order:
            gated(layer, half)
            if half == half_order[0]:
                for s in range(strips):
                    halo_out[layer, :, strip(s)] = padded[s, rows : rows + HALO_ROWS, :].astype(
                        jnp.bfloat16
                    )

        @pl.when(has_next)
        def _():
            halo_copy(layer).start()

        for half in half_order:
            if half == 0:

                @pl.when(has_prev)
                def _():
                    halo_copy(layer).wait_recv()
                    for s in range(strips):
                        padded[s, 0:HALO_ROWS, :] = halo_in[layer, :, strip(s)].astype(jnp.float32)

                @pl.when(spot == 0)
                def _():
                    padded[:, 0:HALO_ROWS, :] = jnp.zeros((strips, HALO_ROWS, LANES), jnp.float32)

            filter_rows(layer, half)
            if half == 0:
                pack_rows(event + 1, 0, row_a)
                pack_rows(event + 1, groups, row_b)
                send_stats(event + 1)
            send_own(q + 1, half)

        def normal(layer=layer, event=event):
            totals = total_stats(event + 1) / model
            centre = totals[0:groups, :]
            spread = jnp.maximum(totals[groups : 2 * groups, :] - centre * centre, 0.0)
            inverse = lax.rsqrt(spread + 1e-05)
            spread_rows(scale_ref, inverse, 0)
            spread_rows(shift_ref, centre * inverse, 0)
            if layer == 0:
                for step in range(1, count):
                    param_copy(step).wait_recv()
            for half in half_order:
                side_wait(2 * layer + 1, z, half)
                mix(layer, z, half)

        def ready(index, half, layer=layer, normal=normal):
            q = 2 * layer + 1
            if index == 0 and half == half_order[0]:
                return
            if index == 0:
                normal()
                for again in half_order:
                    side_wait(q, arrival(0), again)
                    mix(layer, arrival(0), again)
                return
            if index < chips - 2:
                side_wait(q, arrival(index), half)
                mix(layer, arrival(index), half)

        interleave(q + 1, range(base + 2 * pieces, base + 3 * pieces), ready)
        for chunk in range(base + 2 * pieces, base + 3 * pieces):
            finish_chunk(chunk)
        for half in half_order:
            merge(layer, z, half, True)
            for index in range(chips - 2):
                merge(layer, arrival(index), half, False)
        for half in half_order:
            chip = arrival(chips - 2)
            side_wait(q + 1, chip, half)
            mix(layer, chip, half)
            merge(layer, chip, half, False)

            def squares(index, half=half):
                at_rows = tile_at(half * half_rows, index)
                total = jnp.zeros((ROW_TILE, LANES), jnp.float32)
                for s in range(strips):
                    own = acc[0, at_rows, strip(s)].astype(jnp.bfloat16).astype(jnp.float32)
                    total = total + own * own
                row_a[at_rows, :] = total

            loop(half_tiles, squares)
        pack_rows(event + 2, 0, row_a)
        send_stats(event + 2)
        spread_rows(scale_ref, lax.rsqrt(total_stats(event + 2) / model + 1e-06), 0)

        def updated(at_rows, layer=layer):
            branch = acc[0, at_rows, :].astype(jnp.bfloat16).astype(jnp.float32)
            scale = jnp.concatenate([scale_ref[at_rows, :]] * strips, axis=1)
            before = (tok_ref if layer == 0 else stream)[at_rows, :].astype(jnp.float32)
            after = before + branch * scale * post_ref[layer : layer + 1, :]
            after = after.astype(jnp.bfloat16)
            if layer + 1 < layers:
                stream[at_rows, :] = after
            else:
                out_ref[at_rows, :] = after
            return after.astype(jnp.float32)

        if layer + 1 < layers:
            for half in half_order:
                emit_u(layer + 1, half, updated)
                send_own(q + 2, half)
            pack_rows(event + 3, 0, row_a)
            send_stats(event + 3)
        else:
            loop(rows // ROW_TILE, lambda index: updated(tile_at(0, index)))

    for chunk in range(chunk_total):
        for step in range(turns):
            ring_copy(chunk, step, 1).wait_send()
            ring_copy(chunk, step, -1).wait_send()
    for q in range(2 * layers):
        drain(q)
    for step in range(1, count):
        for event in range(3 * layers):
            stat_copy(event, step).wait_send()
        param_copy(step).wait_send()

    @pl.when(has_next)
    def _():
        for layer in range(layers):
            halo_copy(layer).wait_send()


def shards(
    tokens, pre_gain, w_value, w_gate, conv_taps, conv_bias, norm_gain, norm_bias, w_out, post_gain
):
    ring = lax.axis_size("sp")
    count = lax.axis_size("tp")
    chips = count // 2
    layers, depth, width = w_value.shape
    rows = tokens.shape[0]
    pieces = max(1, min(4, depth // 256))
    chunks = 3 * layers * pieces
    strips = width // LANES
    stat_rows = max(8, 2 * rows // LANES)
    param_rows = -(-2 * layers // 8) * 8
    vmem = pl.BlockSpec(memory_space=pltpu.VMEM)
    hbm = pl.BlockSpec(memory_space=pl.ANY)
    dma = pltpu.SemaphoreType.DMA
    scratch = [
        pltpu.VMEM((3 * layers, depth * ring, width), jnp.bfloat16),
        pltpu.VMEM((layers, count, rows, width), jnp.bfloat16),
        pltpu.VMEM((layers, count, rows, width), jnp.bfloat16),
        pltpu.VMEM((count, rows, width), jnp.bfloat16),
        pltpu.VMEM((2, rows, width), jnp.float32),
        pltpu.VMEM((strips, HALO_ROWS + rows, LANES), jnp.float32),
        pltpu.VMEM((rows, LANES), jnp.float32),
        pltpu.VMEM((rows, LANES), jnp.float32),
        pltpu.VMEM((rows, LANES), jnp.float32),
        pltpu.VMEM((rows, LANES), jnp.float32),
        pltpu.VMEM((rows, width), jnp.bfloat16),
        pltpu.VMEM((layers, HALO_ROWS, width), jnp.bfloat16),
        pltpu.VMEM((layers, HALO_ROWS, width), jnp.bfloat16),
        pltpu.VMEM((3 * layers, stat_rows, LANES), jnp.float32),
        pltpu.VMEM((3 * layers, count - 1, stat_rows, LANES), jnp.float32),
        pltpu.VMEM((count, param_rows, width), jnp.float32),
    ]
    scratch += [dma((2 * layers, chips, HALVES))] * 5
    scratch += [dma((chunks, ring // 2))] * 4
    scratch += [dma((chunks,))]
    scratch += [dma((3 * layers, count - 1))] * 2
    scratch += [dma((count - 1,))] * 2
    scratch += [dma((layers,))] * 2
    flops = 2 * rows * model_width(tokens, count) * width * 3 * layers
    return pl.pallas_call(
        functools.partial(module_kernel, ring, count),
        out_shape=jax.ShapeDtypeStruct(tokens.shape, tokens.dtype),
        in_specs=[vmem, vmem, hbm, hbm, hbm] + [vmem] * 5,
        out_specs=vmem,
        scratch_shapes=scratch,
        compiler_params=pltpu.CompilerParams(
            collective_id=0, has_side_effects=True, vmem_limit_bytes=63 * 2**20
        ),
        cost_estimate=pl.CostEstimate(flops=flops, bytes_accessed=flops // 512, transcendentals=0),
        name="modules",
    )(
        tokens,
        pre_gain,
        w_value,
        w_gate,
        w_out,
        conv_taps,
        conv_bias,
        norm_gain,
        norm_bias,
        post_gain,
    )


def model_width(tokens, count):
    return tokens.shape[1] * count


def solution(mesh):
    in_specs = (
        P("sp", "tp"),
        P(),
        P(None, "sp", "tp"),
        P(None, "sp", "tp"),
        P(None, None, "tp"),
        P(None, "tp"),
        P(None, "tp"),
        P(None, "tp"),
        P(None, "sp", "tp"),
        P(None, "tp"),
    )
    out_specs = P("sp", "tp")
    return jax.shard_map(shards, mesh=mesh, in_specs=in_specs, out_specs=out_specs, check_vma=False)
```

profile of v0, /device:TPU:0, one launch (start us, length us, event | category | flops | bytes accessed | tf_op | source)
XLA Modules:
  0.0 267.5 jit_solution(230956670106500438)
XLA Ops:
  0.0 1.6 copy.11.taps_ref
  1.6 264.1 %modules.1 = bf16[512,512]{1,0:T(8,128)(2,1)} custom-call(bf16[512,512]{1,0:T(8,128)(2,1)} %tok_ref.1, f32[2,4096]{1,0:T(2,128)} %pre_ref.1, bf16[2,1024,512]{2,1,0:T(8,128)(2,1)} %value_ref.1, bf16[2,1024,512]{2,1,0:T(8,128)(2,1)} %gate_ref.1, bf16[2,1024,512]{2,1,0:T(8,128)(2,1)} %wout_ref.1, f32[2,31,512]{2,1,0:T(8,128)} %copy.11.taps_ref, ...), custom_call_target="tpu_custom_call" | custom-call | flops 12884901888 | bytes 25165824 | tf_op jit(solution)/shard_map/modules/pallas_call | solution.py:681
  265.6 1.9 copy.13
where the time goes:
time: 268 us
  Pallas kernels  264 us (99%)
  local copies, waits for them, and re-layouts  3.45 us (1%)
    pallas_call x1, Pallas kernels, shards(): pl.pallas_call(functools.partial(module_kernel, ring, count), out_shape=j...  264 us

commit v1 on v0

--- a/solution.py
+++ b/solution.py
@@ -10,9 +10,12 @@
 MESH = pl.DeviceIdType.MESH
 LANES = 128
 HALVES = 2
-AHEAD = 2
+AHEAD = 3
 ROW_TILE = 64
 HALO_ROWS = 32
+LATE_TURNS = (0, 0, 1, 3)
+OUT_TURNS = (1, 2, 4, 5)
+LAST_TURNS = (0, 0, 1, 3)
 
 
 def gray_of(position, count):
@@ -47,17 +50,26 @@
 def module_kernel(
     ring,
     count,
-    tok_ref,
-    pre_ref,
+    tok_hbm,
+    pre_hbm,
     value_ref,
     gate_ref,
     wout_ref,
+    taps_hbm,
+    bias_hbm,
+    ngain_hbm,
+    nbias_hbm,
+    post_hbm,
+    out_ref,
+    tok_ref,
+    pre_ref,
     taps_ref,
     bias_ref,
     ngain_ref,
     nbias_ref,
     post_ref,
-    out_ref,
+    load_sem,
+    tap_rows,
     w_all,
     u_all,
     f_all,
@@ -69,21 +81,32 @@
     scale_ref,
     shift_ref,
     stream,
+    last,
+    last_sem,
     halo_out,
     halo_in,
     stat_out,
     stat_in,
     params,
+    x_all,
+    half_out,
+    half_in,
     z_up,
     z_down,
     z_recv,
     side_send,
     side_recv,
-    ahead_send,
-    ahead_recv,
-    behind_send,
-    behind_recv,
+    ring_send,
+    ring_recv,
+    sub_send,
+    sub_recv,
     own_sem,
+    x_send,
+    x_recv,
+    pass_send,
+    pass_recv,
+    half_send,
+    half_recv,
     stat_send,
     stat_recv,
     par_send,
@@ -94,7 +117,7 @@
     layers, depth, width = value_ref.shape
     rows = tok_ref.shape[0]
     model = width * count
-    tap_count = taps_ref.shape[1]
+    tap_count = taps_ref.shape[0]
     chips = count // 2
     half_rows = rows // HALVES
     strips = width // LANES
@@ -103,6 +126,9 @@
     pieces = max(1, min(4, depth // 256))
     piece = depth // pieces
     turns = ring // 2
+    group = ring // 2
+    group_turns = max(1, group // 2)
+    blocks_held = depth // width
 
     me = lax.axis_index("tp")
     z = me // 2
@@ -114,6 +140,12 @@
     at = position_of(spot, ring)
     ahead = gray_of((at + 1) % ring, ring)
     behind = gray_of((at + ring - 1) % ring, ring)
+    low_bit = spot % 2
+    pair = spot + 1 - 2 * low_bit
+    group_at = position_of(spot // 2, group)
+    group_ahead = 2 * gray_of((group_at + 1) % group, group) + low_bit
+    group_behind = 2 * gray_of((group_at + group - 1) % group, group) + low_bit
+    x_way = at % 2
     has_next = spot < ring - 1
     has_prev = spot > 0
 
@@ -124,6 +156,9 @@
         )
     pl.semaphore_signal(barrier, inc=1, device_id={"sp": ahead}, device_id_type=MESH)
     pl.semaphore_signal(barrier, inc=1, device_id={"sp": behind}, device_id_type=MESH)
+    if group > 2:
+        for member in (group_ahead, group_behind):
+            pl.semaphore_signal(barrier, inc=1, device_id={"sp": member}, device_id_type=MESH)
 
     @pl.when(has_next)
     def _():
@@ -133,8 +168,26 @@
     def _():
         pl.semaphore_signal(barrier, inc=1, device_id={"sp": spot - 1}, device_id_type=MESH)
 
+    loads = [
+        pltpu.make_async_copy(source, there, load_sem.at[number])
+        for number, (source, there) in enumerate(
+            [
+                (tok_hbm, tok_ref),
+                (pre_hbm, pre_ref),
+                (ngain_hbm, ngain_ref),
+                (nbias_hbm, nbias_ref),
+                (taps_hbm, taps_ref),
+                (bias_hbm, bias_ref),
+                (post_hbm, post_ref),
+            ]
+        )
+    ]
+    for load in loads:
+        load.start()
+
     pl.semaphore_wait(
-        barrier, count + 1 + has_next.astype(jnp.int32) + has_prev.astype(jnp.int32)
+        barrier,
+        count + (3 if group > 2 else 1) + has_next.astype(jnp.int32) + has_prev.astype(jnp.int32)
     )
 
     sources = (value_ref, gate_ref, wout_ref)
@@ -144,27 +197,49 @@
         start = owner * depth + (chunk % pieces) * piece + first
         return w_all.at[chunk // pieces, pl.ds(pl.multiple_of(start, size), size), :]
 
-    def ring_copy(chunk, step, sign):
-        owner = gray_of((at + ring - sign * step) % ring, ring)
+    def own_rows(chunk, first, size):
+        projection = chunk // pieces
+        return sources[projection % 3].at[
+            projection // 3, pl.ds((chunk % pieces) * piece + first, size), :
+        ]
+
+    def ring_copy(chunk, step, way):
+        owner = gray_of((at + ring - (1 - 2 * way) * step) % ring, ring)
         last = step == turns - 1
         size = piece // 2 if last else piece
-        first = piece // 2 if last and sign < 0 else 0
+        there = held(chunk, owner, size * way if last else 0, size)
+        return remote(
+            own_rows(chunk, 0, size) if step == 0 else there,
+            there,
+            ring_send.at[way, chunk, step],
+            ring_recv.at[way, chunk, step],
+            "sp",
+            ahead * (1 - way) + behind * way,
+        )
+
+    def sub_copy(chunk, step, way):
+        owner = 2 * gray_of((group_at + group - (1 - 2 * way) * step) % group, group) + low_bit
+        last = step == group_turns - 1
+        size = piece // 2 if last else piece
+        first = size * way if last else 0
         there = held(chunk, owner, first, size)
-        projection = chunk // pieces
-        own = sources[projection % 3].at[
-            projection // 3, pl.ds((chunk % pieces) * piece + first, size), :
-        ]
-        sends, recvs, target = (
-            (ahead_send, ahead_recv, ahead) if sign > 0 else (behind_send, behind_recv, behind)
-        )
         return remote(
-            own if step == 0 else there,
+            own_rows(chunk, first, size) if step == 0 else there,
             there,
-            sends.at[chunk, step],
-            recvs.at[chunk, step],
+            sub_send.at[way, chunk, step],
+            sub_recv.at[way, chunk, step],
             "sp",
-            target,
-        )
+            group_behind if way else group_ahead,
+        )
+
+    def finish_sub(chunk):
+        for step in range(group_turns - 1):
+            for way in range(2):
+                sub_copy(chunk, step, way).wait_recv()
+                sub_copy(chunk, step + 1, way).start()
+        for way in range(2):
+            sub_copy(chunk, group_turns - 1, way).wait_recv()
+        own_copy(chunk).wait()
 
     def own_copy(chunk):
         projection = chunk // pieces
@@ -174,23 +249,27 @@
             own_sem.at[chunk],
         )
 
-    def start_chunk(chunk):
-        if chunk < chunk_total:
-            ring_copy(chunk, 0, 1).start()
-            ring_copy(chunk, 0, -1).start()
-            own_copy(chunk).start()
-
-    def turn_chunk(chunk):
+    started = [3 * pieces]
+
+    def start_until(last):
+        while started[0] <= min(last, chunk_total - 1):
+            for way in range(2):
+                ring_copy(started[0], 0, way).start()
+            own_copy(started[0]).start()
+            started[0] += 1
+
+    def turn_chunk(chunk, most):
         for step in range(turns - 1):
-            ring_copy(chunk, step, 1).wait_recv()
-            ring_copy(chunk, step + 1, 1).start()
-            ring_copy(chunk, step, -1).wait_recv()
-            ring_copy(chunk, step + 1, -1).start()
-        start_chunk(chunk + AHEAD)
+            for way in range(2):
+                ring_copy(chunk, step, way).wait_recv()
+                ring_copy(chunk, step + 1, way).start()
+        if chunk < 5 * pieces - 1:
+            most = min(most, 5 * pieces - 1)
+        start_until(min(chunk + AHEAD, most))
 
     def finish_chunk(chunk):
-        ring_copy(chunk, turns - 1, 1).wait_recv()
-        ring_copy(chunk, turns - 1, -1).wait_recv()
+        for way in range(2):
+            ring_copy(chunk, turns - 1, way).wait_recv()
         own_copy(chunk).wait()
 
     def stage(q):
@@ -223,7 +302,55 @@
             there, there, side_send.at[q, chip, half], side_recv.at[q, chip, half], "tp", partner
         ).wait_recv()
 
+    def mine(block):
+        return (block // blocks_held) % 2 == low_bit
+
+    def x_copy(chip, half):
+        block = 2 * chip + core
+        return remote(
+            part(0, block, half),
+            x_all.at[block, pl.ds(half * half_rows, half_rows), :],
+            x_send.at[chip, half],
+            x_recv.at[chip, half],
+            "sp",
+            pair,
+        )
+
+    def pass_copy(chip, half, block):
+        there = x_all.at[block, pl.ds(half * half_rows, half_rows), :]
+        return remote(
+            there, there, pass_send.at[chip, half], pass_recv.at[chip, half], "tp", partner
+        )
+
+    def cross(chip, half):
+        @pl.when(mine(2 * chip + core))
+        def _():
+            x_copy(chip, half).wait_recv()
+            pass_copy(chip, half, 2 * chip + core).start()
+
+    def cross_wait(chip, half):
+        @pl.when(mine(2 * chip + 1 - core))
+        def _():
+            pass_copy(chip, half, 2 * chip + 1 - core).wait_recv()
+
+    def half_copy(which, half):
+        at_rows = pl.ds(half * half_rows, half_rows)
+        return remote(
+            half_out.at[which, at_rows, :],
+            half_in.at[which, at_rows, :],
+            half_send.at[which, half],
+            half_recv.at[which, half],
+            "sp",
+            pair,
+        )
+
     def send_own(q, half):
+        if q == 0:
+
+            @pl.when(jnp.logical_not(mine(me)))
+            def _():
+                x_copy(z, half).start()
+
         @pl.when(has_up)
         def _():
             up(q, z, half).start()
@@ -244,26 +371,49 @@
         return both * paired + (1 - both) * alone
 
     def relay(q, index, half):
-        chip = arrival(index)
-        there = part(q, 2 * chip + core, half)
-        remote(
-            there, there, z_up.at[q, chip, half], z_recv.at[q, chip, half], "tp", partner
-        ).wait_recv()
-
-        @pl.when((chip < z) & has_up)
-        def _():
-            up(q, chip, half).start()
-
-        @pl.when((chip > z) & has_down)
-        def _():
-            down(q, chip, half).start()
-
-        side(q, chip, half).start()
+        for sign in (-1, 1):
+            chip = z + sign * (index + 1)
+
+            @pl.when((chip >= 0) & (chip < chips))
+            def _():
+                there = part(q, 2 * chip + core, half)
+                remote(
+                    there, there, z_up.at[q, chip, half], z_recv.at[q, chip, half], "tp", partner
+                ).wait_recv()
+
+                if sign < 0:
+
+                    @pl.when(has_up)
+                    def _():
+                        up(q, chip, half).start()
+
+                else:
+
+                    @pl.when(has_down)
+                    def _():
+                        down(q, chip, half).start()
+
+                side(q, chip, half).start()
+                if q == 0:
+
+                    @pl.when(jnp.logical_not(mine(2 * chip + core)))
+                    def _():
+                        x_copy(chip, half).start()
 
     def drain(q):
         def chip_step(chip):
             for half in range(HALVES):
                 side(q, chip, half).wait_send()
+                if q == 0:
+                    for_me = mine(2 * chip + core)
+
+                    @pl.when(for_me)
+                    def _():
+                        pass_copy(chip, half, 2 * chip + core).wait_send()
+
+                    @pl.when(jnp.logical_not(for_me))
+                    def _():
+                        x_copy(chip, half).wait_send()
 
                 @pl.when(has_up & (chip <= z))
                 def _():
@@ -337,24 +487,57 @@
     def columns(index):
         return pl.ds(pl.multiple_of(index * column_tile, column_tile), column_tile)
 
-    def project(layer, which, chunk):
-        offset = (chunk % pieces) * piece
+    def weigh(projection, block, index):
+        rows_of = pl.ds(pl.multiple_of(block * width, width), width)
+        return w_all[projection, rows_of, columns(index)]
+
+    def project_part(which, half, source, keep):
+        at_rows = pl.ds(half * half_rows, half_rows)
 
         def body(index):
             total = None
-            for owner in range(ring):
-                first = owner * depth + offset
-                block, column = first // width, first % width
+            for member in range(group):
+                for inner in range(blocks_held):
+                    block = (2 * member + low_bit) * blocks_held + inner
+                    product = jnp.dot(
+                        source[block, at_rows, :],
+                        weigh(which, block, index),
+                        preferred_element_type=jnp.float32,
+                    )
+                    total = product if total is None else total + product
+            keep(at_rows, columns(index), total)
+
+        loop(width // column_tile, body)
+
+    def project_other(which, half):
+        def keep(at_rows, at_columns, total):
+            half_out[which, at_rows, at_columns] = total.astype(jnp.bfloat16)
+
+        project_part(which, half, x_all, keep)
+        half_copy(which, half).start()
+
+    def project_mine(which, half):
+        def keep(at_rows, at_columns, total):
+            acc[which, at_rows, at_columns] = total
+
+        project_part(which, half, u_all.at[0], keep)
+
+    def project_chip(layer, which, chip, half, first):
+        at_rows = pl.ds(half * half_rows, half_rows)
+
+        def body(index):
+            total = None
+            for c in range(2):
                 product = jnp.dot(
-                    u_all[layer, block, :, column : column + piece],
-                    w_all[3 * layer + which, first : first + piece, columns(index)],
+                    u_all[layer, 2 * chip + c, at_rows, :],
+                    weigh(3 * layer + which, 2 * chip + c, index),
                     preferred_element_type=jnp.float32,
                 )
                 total = product if total is None else total + product
-            if chunk % pieces == 0:
-                acc[which, :, columns(index)] = total
+            if first:
+                acc[which, at_rows, columns(index)] = total
             else:
-                acc[which, :, columns(index)] += total
+                acc[which, at_rows, columns(index)] += total
 
         loop(width // column_tile, body)
 
@@ -363,8 +546,13 @@
             at_rows = tile_at(half * half_rows, index)
             scale = scale_ref[at_rows, :]
             for s in range(strips):
-                value = acc[0, at_rows, strip(s)] * scale
-                gate = acc[1, at_rows, strip(s)] * scale
+                value = acc[0, at_rows, strip(s)]
+                gate = acc[1, at_rows, strip(s)]
+                if layer == 0:
+                    value = value + half_in[0, at_rows, strip(s)].astype(jnp.float32)
+                    gate = gate + half_in[1, at_rows, strip(s)].astype(jnp.float32)
+                value = value * scale
+                gate = gate * scale
                 glu = (value * (0.5 * (1.0 + jnp.tanh(0.5 * gate)))).astype(jnp.bfloat16)
                 padded[
                     s,
@@ -390,7 +578,7 @@
                     total = (
                         total
                         + padded[s, pl.ds(start + tap, ROW_TILE), :]
-                        * taps_ref[layer, tap : tap + 1, strip(s)]
+                        * tap_rows[layer, tap : tap + 1, strip(s)]
                     )
                 f_all[layer, me, at_rows, strip(s)] = total.astype(jnp.bfloat16)
                 first = first + total
@@ -428,11 +616,7 @@
                 block = 2 * chip + c
                 product = jnp.dot(
                     mixed[block, at_rows, :],
-                    w_all[
-                        3 * layer + 2,
-                        pl.ds(pl.multiple_of(block * width, width), width),
-                        columns(index),
-                    ],
+                    weigh(3 * layer + 2, block, index),
                     preferred_element_type=jnp.float32,
                 )
                 total = product if total is None else total + product
@@ -443,8 +627,12 @@
 
         loop(width // column_tile, body)
 
-    for chunk in range(AHEAD):
-        start_chunk(chunk)
+    for chunk in range(2 * pieces):
+        for way in range(2):
+            sub_copy(chunk, 0, way).start()
+        own_copy(chunk).start()
+    for load in loads[:4]:
+        load.wait()
 
     def from_tokens(at_rows):
         return tok_ref[at_rows, :].astype(jnp.float32)
@@ -467,10 +655,17 @@
             lax.rem(me + step, count),
         )
 
+    for chunk in range(2 * pieces, 3 * pieces):
+        ring_copy(chunk, 0, 1 - x_way).start()
+        own_copy(chunk).start()
     pack_rows(0, 0, row_a)
     send_stats(0)
     for step in range(1, count):
         param_copy(step).start()
+
+    def result_copy(half):
+        at_rows = pl.ds(half * half_rows, half_rows)
+        return pltpu.make_async_copy(last.at[at_rows, :], out_ref.at[at_rows, :], last_sem.at[half])
 
     def halo_copy(layer):
         return remote(
@@ -484,46 +679,137 @@
 
     relays = [(index, half) for index in range(chips - 1) for half in half_order]
 
-    def interleave(q, chunks, after):
+    def interleave(q, turns_at, chunks, most, after):
         chunks = list(chunks)
         for number, (index, half) in enumerate(relays):
+            for _ in range(turns_at.count(number)):
+                if chunks:
+                    turn_chunk(chunks.pop(0), most)
             relay(q, index, half)
-            while chunks and len(chunks) * len(relays) > (len(relays) - number - 1) * pieces:
-                turn_chunk(chunks.pop(0))
             after(index, half)
         for chunk in chunks:
-            turn_chunk(chunk)
+            turn_chunk(chunk, most)
+
+    def row_scale(event):
+        norm = lax.rsqrt(total_stats(event) / model + 1e-06)
+        spread_rows(scale_ref, norm, 0)
+
+    def glu_and_halo(layer, half):
+        gated(layer, half)
+        if half == half_order[0]:
+            for s in range(strips):
+                halo_out[layer, :, strip(s)] = padded[s, rows : rows + HALO_ROWS, :].astype(
+                    jnp.bfloat16
+                )
+
+            @pl.when(has_next)
+            def _():
+                halo_copy(layer).start()
+
+    first_out = 2 * pieces
+    second = 3 * pieces
+    midway = 5 * pieces + pieces // 2
+    turns_of = (
+        range(second, second + pieces),
+        range(second + pieces, 5 * pieces),
+        range(5 * pieces, 6 * pieces),
+    )
+
+    def first_projections():
+        crossings = [(z, half) for half in half_order]
+        crossings += [(arrival(index), half) for index, half in relays]
+        paced = list(range(first_out, second))
+        kept = paced[3:]
+        paced = paced[:3]
+
+        def pace():
+            if paced:
+                ring_copy(paced.pop(0), 0, x_way).start()
+
+        pace()
+        pace()
+
+        def after(index, half):
+            pace()
+            if (index, half) != relays[0]:
+                cross(*crossings.pop(0))
+
+        interleave(0, (), (), 0, after)
+        for half in half_order:
+            side_wait(0, z, half)
+            for index in range(chips - 1):
+                side_wait(0, arrival(index), half)
+        row_scale(0)
+        for load in loads[4:]:
+            load.wait()
+        for each in range(layers):
+            for tap in range(tap_count):
+                tap_rows[each, tap : tap + 1, :] = taps_ref[tap, each : each + 1, :]
+        for which in range(2):
+            for chunk in range(which * pieces, (which + 1) * pieces):
+                finish_sub(chunk)
+            for half in half_order:
+                if which == 0:
+                    while crossings and crossings[0][1] == half or len(crossings) > 1:
+                        cross(*crossings.pop(0))
+                    for index in range(-1, chips - 1):
+                        cross_wait(z if index < 0 else arrival(index), half)
+                project_other(which, half)
+            if which == 1:
+                for chunk in paced + kept:
+                    ring_copy(chunk, 0, x_way).start()
+            for half in half_order:
+                project_mine(which, half)
+        for chunk in range(first_out, first_out + pieces // 2):
+            turn_chunk(chunk, 0)
+        for half in half_order:
+            for which in range(2):
+                half_copy(which, half).wait_recv()
+            glu_and_halo(0, half)
+    def later_projections(layer):
+        base = 3 * layer * pieces
+
+        def chip_of(index):
+            return z if index < 0 else arrival(index)
+
+        def take(which, index, half):
+            project_chip(layer, which, chip_of(index), half, index < 0)
+
+        def after(index, half):
+            if half == half_order[-1] and index < chips - 2:
+                if index == 0:
+                    for chunk in range(base, base + pieces):
+                        finish_chunk(chunk)
+                for done in [-1, 0] if index == 0 else [index]:
+                    for each in half_order:
+                        side_wait(2 * layer, chip_of(done), each)
+                        take(0, done, each)
+            if index == chips - 2:
+                if half == half_order[0]:
+                    for chunk in range(base + pieces, base + 2 * pieces):
+                        finish_chunk(chunk)
+                    for done in range(-1, chips - 2):
+                        for each in half_order:
+                            take(1, done, each)
+                else:
+                    row_scale(3 * layer)
+                side_wait(2 * layer, chip_of(index), half)
+                take(0, index, half)
+                take(1, index, half)
+
+        interleave(2 * layer, LATE_TURNS, turns_of[1], midway - 1, after)
+        for half in half_order:
+            glu_and_halo(layer, half)
+        start_until(midway + AHEAD - 1)
 
     for layer in range(layers):
-        base = 3 * layer * pieces
         q = 2 * layer
         event = 3 * layer
-        interleave(q, range(base, base + pieces), lambda index, half: None)
-        for half in half_order:
-            side_wait(q, z, half)
-            for index in range(chips - 1):
-                side_wait(q, arrival(index), half)
-        norm = lax.rsqrt(total_stats(event) / model + 1e-06)
-        spread_rows(scale_ref, norm, 0)
-        for chunk in range(base, base + pieces):
-            finish_chunk(chunk)
-            project(layer, 0, chunk)
-            turn_chunk(chunk + pieces)
-        for chunk in range(base + pieces, base + 2 * pieces):
-            finish_chunk(chunk)
-            project(layer, 1, chunk)
-
-        for half in half_order:
-            gated(layer, half)
-            if half == half_order[0]:
-                for s in range(strips):
-                    halo_out[layer, :, strip(s)] = padded[s, rows : rows + HALO_ROWS, :].astype(
-                        jnp.bfloat16
-                    )
-
-        @pl.when(has_next)
-        def _():
-            halo_copy(layer).start()
+        base = 3 * layer * pieces
+        if layer == 0:
+            first_projections()
+        else:
+            later_projections(layer)
 
         for half in half_order:
             if half == 0:
@@ -544,6 +830,10 @@
                 pack_rows(event + 1, groups, row_b)
                 send_stats(event + 1)
             send_own(q + 1, half)
+
+        if layer == 0:
+            for chunk in range(first_out + pieces // 2, second):
+                turn_chunk(chunk, midway - 1)
 
         def normal(layer=layer, event=event):
             totals = total_stats(event + 1) / model
@@ -569,23 +859,25 @@
                     side_wait(q, arrival(0), again)
                     mix(layer, arrival(0), again)
                 return
-            if index < chips - 2:
-                side_wait(q, arrival(index), half)
-                mix(layer, arrival(index), half)
-
-        interleave(q + 1, range(base + 2 * pieces, base + 3 * pieces), ready)
-        for chunk in range(base + 2 * pieces, base + 3 * pieces):
-            finish_chunk(chunk)
+            if index == chips - 2 and half == half_order[0]:
+                for chunk in range((3 * layer + 2) * pieces, (3 * layer + 3) * pieces):
+                    finish_chunk(chunk)
+                for each in half_order:
+                    for done in range(-1, chips - 2):
+                        merge(layer, z if done < 0 else arrival(done), each, done < 0)
+            side_wait(q, arrival(index), half)
+            mix(layer, arrival(index), half)
+            if index == chips - 2:
+                merge(layer, arrival(index), half, False)
+
+        interleave(
+            q + 1,
+            LAST_TURNS if layer else OUT_TURNS,
+            turns_of[2] if layer else turns_of[0],
+            chunk_total if layer else midway - 1,
+            ready,
+        )
         for half in half_order:
-            merge(layer, z, half, True)
-            for index in range(chips - 2):
-                merge(layer, arrival(index), half, False)
-        for half in half_order:
-            chip = arrival(chips - 2)
-            side_wait(q + 1, chip, half)
-            mix(layer, chip, half)
-            merge(layer, chip, half, False)
-
             def squares(index, half=half):
                 at_rows = tile_at(half * half_rows, index)
                 total = jnp.zeros((ROW_TILE, LANES), jnp.float32)
@@ -608,7 +900,7 @@
             if layer + 1 < layers:
                 stream[at_rows, :] = after
             else:
-                out_ref[at_rows, :] = after
+                last[at_rows, :] = after
             return after.astype(jnp.float32)
 
         if layer + 1 < layers:
@@ -618,12 +910,20 @@
             pack_rows(event + 3, 0, row_a)
             send_stats(event + 3)
         else:
-            loop(rows // ROW_TILE, lambda index: updated(tile_at(0, index)))
-
-    for chunk in range(chunk_total):
-        for step in range(turns):
-            ring_copy(chunk, step, 1).wait_send()
-            ring_copy(chunk, step, -1).wait_send()
+            for half in half_order:
+                loop(half_tiles, lambda index, half=half: updated(tile_at(half * half_rows, index)))
+                result_copy(half).start()
+
+    for way in range(2):
+        for chunk in range(2 * pieces):
+            for step in range(group_turns):
+                sub_copy(chunk, step, way).wait_send()
+        for chunk in range(2 * pieces, chunk_total):
+            for step in range(turns):
+                ring_copy(chunk, step, way).wait_send()
+    for which in range(2):
+        for half in range(HALVES):
+            half_copy(which, half).wait_send()
     for q in range(2 * layers):
         drain(q)
     for step in range(1, count):
@@ -635,6 +935,9 @@
     def _():
         for layer in range(layers):
             halo_copy(layer).wait_send()
+
+    for half in half_order:
+        result_copy(half).wait()
 
 
 def shards(
@@ -650,10 +953,14 @@
     strips = width // LANES
     stat_rows = max(8, 2 * rows // LANES)
     param_rows = -(-2 * layers // 8) * 8
-    vmem = pl.BlockSpec(memory_space=pltpu.VMEM)
     hbm = pl.BlockSpec(memory_space=pl.ANY)
     dma = pltpu.SemaphoreType.DMA
-    scratch = [
+    taps = jnp.transpose(conv_taps, (1, 0, 2))
+    loaded = [tokens, pre_gain, taps, conv_bias, norm_gain, norm_bias, post_gain]
+    scratch = [pltpu.VMEM(array.shape, array.dtype) for array in loaded]
+    scratch += [dma((len(loaded),))]
+    scratch += [pltpu.VMEM(conv_taps.shape, conv_taps.dtype)]
+    scratch += [
         pltpu.VMEM((3 * layers, depth * ring, width), jnp.bfloat16),
         pltpu.VMEM((layers, count, rows, width), jnp.bfloat16),
         pltpu.VMEM((layers, count, rows, width), jnp.bfloat16),
@@ -665,15 +972,23 @@
         pltpu.VMEM((rows, LANES), jnp.float32),
         pltpu.VMEM((rows, LANES), jnp.float32),
         pltpu.VMEM((rows, width), jnp.bfloat16),
+        pltpu.VMEM((rows, width), jnp.bfloat16),
+        dma((HALVES,)),
         pltpu.VMEM((layers, HALO_ROWS, width), jnp.bfloat16),
         pltpu.VMEM((layers, HALO_ROWS, width), jnp.bfloat16),
         pltpu.VMEM((3 * layers, stat_rows, LANES), jnp.float32),
         pltpu.VMEM((3 * layers, count - 1, stat_rows, LANES), jnp.float32),
         pltpu.VMEM((count, param_rows, width), jnp.float32),
+        pltpu.VMEM((count, rows, width), jnp.bfloat16),
+        pltpu.VMEM((2, rows, width), jnp.bfloat16),
+        pltpu.VMEM((2, rows, width), jnp.bfloat16),
     ]
     scratch += [dma((2 * layers, chips, HALVES))] * 5
-    scratch += [dma((chunks, ring // 2))] * 4
+    scratch += [dma((2, chunks, ring // 2))] * 2
+    scratch += [dma((2, 2 * pieces, max(1, ring // 4)))] * 2
     scratch += [dma((chunks,))]
+    scratch += [dma((chips, HALVES))] * 4
+    scratch += [dma((2, HALVES))] * 2
     scratch += [dma((3 * layers, count - 1))] * 2
     scratch += [dma((count - 1,))] * 2
     scratch += [dma((layers,))] * 2
@@ -681,8 +996,8 @@
     return pl.pallas_call(
         functools.partial(module_kernel, ring, count),
         out_shape=jax.ShapeDtypeStruct(tokens.shape, tokens.dtype),
-        in_specs=[vmem, vmem, hbm, hbm, hbm] + [vmem] * 5,
-        out_specs=vmem,
+        in_specs=[hbm] * 10,
+        out_specs=hbm,
         scratch_shapes=scratch,
         compiler_params=pltpu.CompilerParams(
             collective_id=0, has_side_effects=True, vmem_limit_bytes=63 * 2**20
@@ -695,7 +1010,7 @@
         w_value,
         w_gate,
         w_out,
-        conv_taps,
+        taps,
         conv_bias,
         norm_gain,
         norm_bias,

time: 268 us -> 216 us (0.81)
  Pallas kernels: 264 us -> 214 us
    pallas_call x1, Pallas kernels: 264 us -> 214 us  [shards(): pl.pallas_call(functools.partial(module_kernel, ring, count), out_shape=j...]
where the time goes in v1:
time: 216 us
  Pallas kernels  214 us (99%)
    pallas_call x1, Pallas kernels, shards(): pl.pallas_call(functools.partial(module_kernel, ring, count), out_shape=j...  214 us

profile of v1, /device:TPU:0, one launch (start us, length us, event | category | flops | bytes accessed | tf_op | source)
XLA Modules:
  0.0 215.7 jit_solution(14879886002519986367)
XLA Ops:
  0.0 213.8 %modules.1 = bf16[512,512]{1,0:T(8,128)(2,1)} custom-call(bf16[512,512]{1,0:T(8,128)(2,1)} %tok_hbm.1, f32[2,4096]{1,0:T(2,128)} %pre_hbm.1, bf16[2,1024,512]{2,1,0:T(8,128)(2,1)} %value_ref.1, bf16[2,1024,512]{2,1,0:T(8,128)(2,1)} %gate_ref.1, bf16[2,1024,512]{2,1,0:T(8,128)(2,1)} %wout_ref.1, f32[31,2,512]{2,1,0:T(2,128)} %bitcast.1, f32[2,512]{1,0:T(2,128)} %bias_hbm.1, ...), custom_call_target="tpu_custom_call" | custom-call | flops 12884901888 | bytes 25165824 | tf_op jit(solution)/shard_map/modules/pallas_call | solution.py:996
  213.8 1.9 copy.12

commit v2 on v1

--- a/solution.py
+++ b/solution.py
@@ -11,11 +11,11 @@
 LANES = 128
 HALVES = 2
 AHEAD = 3
-ROW_TILE = 64
+TILE_MOST = 112
 HALO_ROWS = 32
-LATE_TURNS = (0, 0, 1, 3)
-OUT_TURNS = (1, 2, 4, 5)
-LAST_TURNS = (0, 0, 1, 3)
+LATE_TURNS = (0, 1, 3, 5)
+OUT_TURNS = (2, 3, 4)
+LAST_TURNS = (0, 1, 2, 4)
 
 
 def gray_of(position, count):
@@ -119,7 +119,6 @@
     model = width * count
     tap_count = taps_ref.shape[0]
     chips = count // 2
-    half_rows = rows // HALVES
     strips = width // LANES
     groups = rows // LANES
     half_order = tuple(reversed(range(HALVES)))
@@ -129,6 +128,23 @@
     group = ring // 2
     group_turns = max(1, group // 2)
     blocks_held = depth // width
+
+    def bounds(q, half):
+        split = rows // 2 - HALO_ROWS * (layers - (q + 1) // 2)
+        return (split, rows - split) if half else (0, split)
+
+    def rows_of(q, half):
+        start, size = bounds(q, half)
+        return pl.ds(start, size)
+
+    def groups_of(q, half):
+        start, size = bounds(q, half)
+        return start // LANES, -(-(start + size) // LANES)
+
+    def tiles(q, half, body):
+        start, size = bounds(q, half)
+        tile = max(t for t in range(16, TILE_MOST + 1, 16) if size % t == 0)
+        loop(size // tile, lambda index: body(pl.multiple_of(start + index * tile, 16), tile))
 
     me = lax.axis_index("tp")
     z = me // 2
@@ -211,8 +227,8 @@
         return remote(
             own_rows(chunk, 0, size) if step == 0 else there,
             there,
-            ring_send.at[way, chunk, step],
-            ring_recv.at[way, chunk, step],
+            ring_send.at[chunk - 2 * pieces],
+            ring_recv.at[chunk - 2 * pieces, step],
             "sp",
             ahead * (1 - way) + behind * way,
         )
@@ -226,7 +242,7 @@
         return remote(
             own_rows(chunk, first, size) if step == 0 else there,
             there,
-            sub_send.at[way, chunk, step],
+            sub_send.at[0],
             sub_recv.at[way, chunk, step],
             "sp",
             group_behind if way else group_ahead,
@@ -239,15 +255,22 @@
                 sub_copy(chunk, step + 1, way).start()
         for way in range(2):
             sub_copy(chunk, group_turns - 1, way).wait_recv()
-        own_copy(chunk).wait()
-
-    def own_copy(chunk):
-        projection = chunk // pieces
+        if chunk % pieces == 0:
+            own_copy(chunk // pieces).wait()
+
+    def own_copy(projection):
         return pltpu.make_async_copy(
-            sources[projection % 3].at[projection // 3, pl.ds((chunk % pieces) * piece, piece), :],
-            held(chunk, spot, 0, piece),
-            own_sem.at[chunk],
-        )
+            sources[projection % 3].at[projection // 3],
+            w_all.at[projection, pl.ds(pl.multiple_of(spot * depth, depth), depth), :],
+            own_sem.at[projection],
+        )
+
+    def await_bytes(ref, sem):
+        pltpu.make_async_copy(ref, ref, sem).wait()
+
+    def ring_arrived(chunk, step):
+        size = 2 * piece if step < turns - 1 else piece
+        await_bytes(w_all.at[0, 0:size, :], ring_recv.at[chunk - 2 * pieces, step])
 
     started = [3 * pieces]
 
@@ -255,51 +278,50 @@
         while started[0] <= min(last, chunk_total - 1):
             for way in range(2):
                 ring_copy(started[0], 0, way).start()
-            own_copy(started[0]).start()
             started[0] += 1
 
     def turn_chunk(chunk, most):
         for step in range(turns - 1):
+            ring_arrived(chunk, step)
             for way in range(2):
-                ring_copy(chunk, step, way).wait_recv()
                 ring_copy(chunk, step + 1, way).start()
         if chunk < 5 * pieces - 1:
             most = min(most, 5 * pieces - 1)
         start_until(min(chunk + AHEAD, most))
 
     def finish_chunk(chunk):
-        for way in range(2):
-            ring_copy(chunk, turns - 1, way).wait_recv()
-        own_copy(chunk).wait()
+        ring_arrived(chunk, turns - 1)
+        if chunk % pieces == 0:
+            own_copy(chunk // pieces).wait()
 
     def stage(q):
         return (u_all if q % 2 == 0 else f_all).at[q // 2]
 
     def part(q, block, half):
-        return stage(q).at[block, pl.ds(half * half_rows, half_rows), :]
+        return stage(q).at[block, rows_of(q, half), :]
 
     def up(q, chip, half):
         there = part(q, 2 * chip + core, half)
         return remote(
-            there, there, z_up.at[q, chip, half], z_recv.at[q, chip, half], "tp", me + 2
+            there, there, z_up.at[q], z_recv.at[q, chip, half], "tp", me + 2
         )
 
     def down(q, chip, half):
         there = part(q, 2 * chip + core, half)
         return remote(
-            there, there, z_down.at[q, chip, half], z_recv.at[q, chip, half], "tp", me - 2
+            there, there, z_down.at[q], z_recv.at[q, chip, half], "tp", me - 2
         )
 
     def side(q, chip, half):
         there = part(q, 2 * chip + core, half)
         return remote(
-            there, there, side_send.at[q, chip, half], side_recv.at[q, chip, half], "tp", partner
+            there, there, side_send.at[q], side_recv.at[q, chip, half], "tp", partner
         )
 
     def side_wait(q, chip, half):
         there = part(q, 2 * chip + 1 - core, half)
         remote(
-            there, there, side_send.at[q, chip, half], side_recv.at[q, chip, half], "tp", partner
+            there, there, side_send.at[q], side_recv.at[q, chip, half], "tp", partner
         ).wait_recv()
 
     def mine(block):
@@ -309,7 +331,7 @@
         block = 2 * chip + core
         return remote(
             part(0, block, half),
-            x_all.at[block, pl.ds(half * half_rows, half_rows), :],
+            x_all.at[block, rows_of(0, half), :],
             x_send.at[chip, half],
             x_recv.at[chip, half],
             "sp",
@@ -317,7 +339,7 @@
         )
 
     def pass_copy(chip, half, block):
-        there = x_all.at[block, pl.ds(half * half_rows, half_rows), :]
+        there = x_all.at[block, rows_of(0, half), :]
         return remote(
             there, there, pass_send.at[chip, half], pass_recv.at[chip, half], "tp", partner
         )
@@ -334,7 +356,7 @@
             pass_copy(chip, half, 2 * chip + 1 - core).wait_recv()
 
     def half_copy(which, half):
-        at_rows = pl.ds(half * half_rows, half_rows)
+        at_rows = rows_of(0, half)
         return remote(
             half_out.at[which, at_rows, :],
             half_in.at[which, at_rows, :],
@@ -378,7 +400,7 @@
             def _():
                 there = part(q, 2 * chip + core, half)
                 remote(
-                    there, there, z_up.at[q, chip, half], z_recv.at[q, chip, half], "tp", partner
+                    there, there, z_up.at[q], z_recv.at[q, chip, half], "tp", partner
                 ).wait_recv()
 
                 if sign < 0:
@@ -401,42 +423,41 @@
                         x_copy(chip, half).start()
 
     def drain(q):
-        def chip_step(chip):
-            for half in range(HALVES):
-                side(q, chip, half).wait_send()
-                if q == 0:
-                    for_me = mine(2 * chip + core)
-
-                    @pl.when(for_me)
+        await_bytes(stage(q).at[0:chips], side_send.at[q])
+        for chip in range(chips):
+
+            @pl.when(has_up & (z == chip))
+            def _():
+                await_bytes(stage(q).at[0 : chip + 1], z_up.at[q])
+
+            @pl.when(has_down & (z == chip))
+            def _():
+                await_bytes(stage(q).at[0 : chips - chip], z_down.at[q])
+
+        if q == 0:
+            for chip in range(chips):
+                for half in range(HALVES):
+
+                    @pl.when(mine(2 * chip + core))
                     def _():
                         pass_copy(chip, half, 2 * chip + core).wait_send()
 
-                    @pl.when(jnp.logical_not(for_me))
+                    @pl.when(jnp.logical_not(mine(2 * chip + core)))
                     def _():
                         x_copy(chip, half).wait_send()
-
-                @pl.when(has_up & (chip <= z))
-                def _():
-                    up(q, chip, half).wait_send()
-
-                @pl.when(has_down & (chip >= z))
-                def _():
-                    down(q, chip, half).wait_send()
-
-        loop(chips, chip_step)
 
     def stat_copy(event, step):
         return remote(
             stat_out.at[event],
             stat_in.at[event, step - 1],
-            stat_send.at[event, step - 1],
+            stat_send.at[0],
             stat_recv.at[event, step - 1],
             "tp",
             lax.rem(me + step, count),
         )
 
-    def pack_rows(event, base, ref):
-        for group in range(groups):
+    def pack_rows(event, base, ref, first=0, last=groups):
+        for group in range(first, last):
             turned = ref[group * LANES : (group + 1) * LANES, :].T
             stat_out[event, base + group : base + group + 1, :] = jnp.sum(
                 turned, axis=0, keepdims=True
@@ -453,8 +474,8 @@
             total = total + stat_in[event, step - 1]
         return total
 
-    def spread_rows(ref, packed, base):
-        for group in range(groups):
+    def spread_rows(ref, packed, base, first=0, last=groups):
+        for group in range(first, last):
             line = packed[base + group : base + group + 1, :]
             ref[group * LANES : (group + 1) * LANES, :] = jnp.broadcast_to(
                 line, (LANES, LANES)
@@ -463,16 +484,11 @@
     def strip(index):
         return slice(index * LANES, (index + 1) * LANES)
 
-    def tile_at(base, index):
-        return pl.ds(pl.multiple_of(base + index * ROW_TILE, ROW_TILE), ROW_TILE)
-
-    half_tiles = half_rows // ROW_TILE
-
     def emit_u(layer, half, source):
-        def body(index):
-            at_rows = tile_at(half * half_rows, index)
+        def body(start, tile):
+            at_rows = pl.ds(start, tile)
             values = source(at_rows)
-            squares = jnp.zeros((ROW_TILE, LANES), jnp.float32)
+            squares = jnp.zeros((tile, LANES), jnp.float32)
             for s in range(strips):
                 own = values[:, strip(s)]
                 squares = squares + own * own
@@ -480,7 +496,7 @@
             gain = pre_ref[layer : layer + 1, pl.ds(pl.multiple_of(me * width, width), width)]
             u_all[layer, me, at_rows, :] = (values * gain).astype(jnp.bfloat16)
 
-        loop(half_tiles, body)
+        tiles(2 * layer, half, body)
 
     column_tile = min(256, width)
 
@@ -488,11 +504,11 @@
         return pl.ds(pl.multiple_of(index * column_tile, column_tile), column_tile)
 
     def weigh(projection, block, index):
-        rows_of = pl.ds(pl.multiple_of(block * width, width), width)
-        return w_all[projection, rows_of, columns(index)]
+        at_block = pl.ds(pl.multiple_of(block * width, width), width)
+        return w_all[projection, at_block, columns(index)]
 
     def project_part(which, half, source, keep):
-        at_rows = pl.ds(half * half_rows, half_rows)
+        at_rows = rows_of(0, half)
 
         def body(index):
             total = None
@@ -523,7 +539,7 @@
         project_part(which, half, u_all.at[0], keep)
 
     def project_chip(layer, which, chip, half, first):
-        at_rows = pl.ds(half * half_rows, half_rows)
+        at_rows = rows_of(2 * layer, half)
 
         def body(index):
             total = None
@@ -541,9 +557,29 @@
 
         loop(width // column_tile, body)
 
+    def project_chunk(layer, which, chunk, at_rows):
+        offset = (chunk % pieces) * piece
+
+        def body(index):
+            total = None
+            for owner in range(ring):
+                first = owner * depth + offset
+                product = jnp.dot(
+                    u_all[layer, first // width, at_rows, first % width : first % width + piece],
+                    w_all[3 * layer + which, first : first + piece, columns(index)],
+                    preferred_element_type=jnp.float32,
+                )
+                total = product if total is None else total + product
+            if chunk % pieces == 0:
+                acc[which, at_rows, columns(index)] = total
+            else:
+                acc[which, at_rows, columns(index)] += total
+
+        loop(width // column_tile, body)
+
     def gated(layer, half):
-        def body(index):
-            at_rows = tile_at(half * half_rows, index)
+        def body(start, tile):
+            at_rows = pl.ds(start, tile)
             scale = scale_ref[at_rows, :]
             for s in range(strips):
                 value = acc[0, at_rows, strip(s)]
@@ -554,30 +590,26 @@
                 value = value * scale
                 gate = gate * scale
                 glu = (value * (0.5 * (1.0 + jnp.tanh(0.5 * gate)))).astype(jnp.bfloat16)
-                padded[
-                    s,
-                    pl.ds(
-                        pl.multiple_of(HALO_ROWS + half * half_rows + index * ROW_TILE, 8), ROW_TILE
-                    ),
-                    :,
-                ] = glu.astype(jnp.float32)
-
-        loop(half_tiles, body)
+                padded[s, pl.ds(pl.multiple_of(HALO_ROWS + start, 8), tile), :] = glu.astype(
+                    jnp.float32
+                )
+
+        tiles(2 * layer, half, body)
 
     def filter_rows(layer, half):
-        def body(index):
-            at_rows = tile_at(half * half_rows, index)
-            start = half * half_rows + index * ROW_TILE + HALO_ROWS - (tap_count - 1)
-            first = jnp.zeros((ROW_TILE, LANES), jnp.float32)
-            second = jnp.zeros((ROW_TILE, LANES), jnp.float32)
+        def body(start, tile):
+            at_rows = pl.ds(start, tile)
+            oldest = start + HALO_ROWS - (tap_count - 1)
+            first = jnp.zeros((tile, LANES), jnp.float32)
+            second = jnp.zeros((tile, LANES), jnp.float32)
             for s in range(strips):
-                total = jnp.zeros((ROW_TILE, LANES), jnp.float32) + bias_ref[
+                total = jnp.zeros((tile, LANES), jnp.float32) + bias_ref[
                     layer : layer + 1, strip(s)
                 ]
                 for tap in range(tap_count):
                     total = (
                         total
-                        + padded[s, pl.ds(start + tap, ROW_TILE), :]
+                        + padded[s, pl.ds(oldest + tap, tile), :]
                         * tap_rows[layer, tap : tap + 1, strip(s)]
                     )
                 f_all[layer, me, at_rows, strip(s)] = total.astype(jnp.bfloat16)
@@ -586,7 +618,7 @@
             row_a[at_rows, :] = first
             row_b[at_rows, :] = second
 
-        loop(half_tiles, body)
+        tiles(2 * layer + 1, half, body)
 
     def mix(layer, chip, half):
         for c in range(2):
@@ -594,8 +626,8 @@
             gains = params[block, 2 * layer : 2 * layer + 1, :]
             biases = params[block, 2 * layer + 1 : 2 * layer + 2, :]
 
-            def body(index):
-                at_rows = tile_at(half * half_rows, index)
+            def body(start, tile):
+                at_rows = pl.ds(start, tile)
                 scale = scale_ref[at_rows, :]
                 shift = shift_ref[at_rows, :]
                 for s in range(strips):
@@ -605,10 +637,10 @@
                         shaped * (0.5 * (1.0 + jnp.tanh(0.5 * shaped)))
                     ).astype(jnp.bfloat16)
 
-            loop(half_tiles, body)
+            tiles(2 * layer + 1, half, body)
 
     def merge(layer, chip, half, first):
-        at_rows = pl.ds(half * half_rows, half_rows)
+        at_rows = rows_of(2 * layer + 1, half)
 
         def body(index):
             total = None
@@ -630,7 +662,6 @@
     for chunk in range(2 * pieces):
         for way in range(2):
             sub_copy(chunk, 0, way).start()
-        own_copy(chunk).start()
     for load in loads[:4]:
         load.wait()
 
@@ -649,7 +680,7 @@
         return remote(
             params.at[me],
             params.at[me],
-            par_send.at[step - 1],
+            par_send.at[0],
             par_recv.at[step - 1],
             "tp",
             lax.rem(me + step, count),
@@ -657,14 +688,15 @@
 
     for chunk in range(2 * pieces, 3 * pieces):
         ring_copy(chunk, 0, 1 - x_way).start()
-        own_copy(chunk).start()
+    for projection in range(3 * layers):
+        own_copy(projection).start()
     pack_rows(0, 0, row_a)
     send_stats(0)
     for step in range(1, count):
         param_copy(step).start()
 
     def result_copy(half):
-        at_rows = pl.ds(half * half_rows, half_rows)
+        at_rows = rows_of(2 * layers - 1, half)
         return pltpu.make_async_copy(last.at[at_rows, :], out_ref.at[at_rows, :], last_sem.at[half])
 
     def halo_copy(layer):
@@ -706,12 +738,33 @@
             def _():
                 halo_copy(layer).start()
 
+    def emit_f(layer, half):
+        if half == 0:
+
+            @pl.when(has_prev)
+            def _():
+                halo_copy(layer).wait_recv()
+                for s in range(strips):
+                    padded[s, 0:HALO_ROWS, :] = halo_in[layer, :, strip(s)].astype(jnp.float32)
+
+            @pl.when(spot == 0)
+            def _():
+                padded[:, 0:HALO_ROWS, :] = jnp.zeros((strips, HALO_ROWS, LANES), jnp.float32)
+
+        filter_rows(layer, half)
+        if half == 0:
+            event = 4 * layer + 1
+            pack_rows(event, 0, row_a)
+            pack_rows(event, groups, row_b)
+            send_stats(event)
+        send_own(2 * layer + 1, half)
+
     first_out = 2 * pieces
     second = 3 * pieces
-    midway = 5 * pieces + pieces // 2
+    midway = 5 * pieces + 1
     turns_of = (
-        range(second, second + pieces),
-        range(second + pieces, 5 * pieces),
+        range(second - 1, second + pieces - 1),
+        range(second + pieces - 1, 5 * pieces),
         range(5 * pieces, 6 * pieces),
     )
 
@@ -755,17 +808,22 @@
                     for index in range(-1, chips - 1):
                         cross_wait(z if index < 0 else arrival(index), half)
                 project_other(which, half)
-            if which == 1:
-                for chunk in paced + kept:
-                    ring_copy(chunk, 0, x_way).start()
             for half in half_order:
                 project_mine(which, half)
         for chunk in range(first_out, first_out + pieces // 2):
             turn_chunk(chunk, 0)
+        turned = list(range(first_out + pieces // 2, second - 1))
         for half in half_order:
             for which in range(2):
                 half_copy(which, half).wait_recv()
             glu_and_halo(0, half)
+            if half == half_order[0]:
+                for chunk in paced + kept:
+                    ring_copy(chunk, 0, x_way).start()
+            emit_f(0, half)
+            if half == half_order[0]:
+                for chunk in turned:
+                    turn_chunk(chunk, midway - 1)
     def later_projections(layer):
         base = 3 * layer * pieces
 
@@ -776,64 +834,47 @@
             project_chip(layer, which, chip_of(index), half, index < 0)
 
         def after(index, half):
-            if half == half_order[-1] and index < chips - 2:
-                if index == 0:
+            if half == half_order[-1] and 0 < index < chips - 2:
+                if index == 1:
                     for chunk in range(base, base + pieces):
                         finish_chunk(chunk)
-                for done in [-1, 0] if index == 0 else [index]:
+                for done in [-1, 0, 1] if index == 1 else [index]:
                     for each in half_order:
                         side_wait(2 * layer, chip_of(done), each)
                         take(0, done, each)
-            if index == chips - 2:
-                if half == half_order[0]:
-                    for chunk in range(base + pieces, base + 2 * pieces):
-                        finish_chunk(chunk)
-                    for done in range(-1, chips - 2):
-                        for each in half_order:
-                            take(1, done, each)
-                else:
-                    row_scale(3 * layer)
-                side_wait(2 * layer, chip_of(index), half)
-                take(0, index, half)
-                take(1, index, half)
-
         interleave(2 * layer, LATE_TURNS, turns_of[1], midway - 1, after)
         for half in half_order:
+            side_wait(2 * layer, chip_of(chips - 2), half)
+            take(0, chips - 2, half)
+        row_scale(4 * layer)
+        for chunk in range(base + pieces, base + 2 * pieces - 1):
+            finish_chunk(chunk)
+            project_chunk(layer, 1, chunk, slice(0, rows))
+        finish_chunk(base + 2 * pieces - 1)
+        for half in half_order:
+            start, size = bounds(2 * layer, half)
+            project_chunk(layer, 1, base + 2 * pieces - 1, slice(start, start + size))
             glu_and_halo(layer, half)
-        start_until(midway + AHEAD - 1)
+            if half == half_order[0]:
+                start_until(midway + AHEAD - 1)
+            emit_f(layer, half)
+
+    def squares(start, tile):
+        at_rows = pl.ds(start, tile)
+        total = jnp.zeros((tile, LANES), jnp.float32)
+        for s in range(strips):
+            own = acc[0, at_rows, strip(s)].astype(jnp.bfloat16).astype(jnp.float32)
+            total = total + own * own
+        row_b[at_rows, :] = total
 
     for layer in range(layers):
         q = 2 * layer
-        event = 3 * layer
+        event = 4 * layer
         base = 3 * layer * pieces
         if layer == 0:
             first_projections()
         else:
             later_projections(layer)
-
-        for half in half_order:
-            if half == 0:
-
-                @pl.when(has_prev)
-                def _():
-                    halo_copy(layer).wait_recv()
-                    for s in range(strips):
-                        padded[s, 0:HALO_ROWS, :] = halo_in[layer, :, strip(s)].astype(jnp.float32)
-
-                @pl.when(spot == 0)
-                def _():
-                    padded[:, 0:HALO_ROWS, :] = jnp.zeros((strips, HALO_ROWS, LANES), jnp.float32)
-
-            filter_rows(layer, half)
-            if half == 0:
-                pack_rows(event + 1, 0, row_a)
-                pack_rows(event + 1, groups, row_b)
-                send_stats(event + 1)
-            send_own(q + 1, half)
-
-        if layer == 0:
-            for chunk in range(first_out + pieces // 2, second):
-                turn_chunk(chunk, midway - 1)
 
         def normal(layer=layer, event=event):
             totals = total_stats(event + 1) / model
@@ -869,6 +910,9 @@
             mix(layer, arrival(index), half)
             if index == chips - 2:
                 merge(layer, arrival(index), half, False)
+                tiles(q, half, squares)
+                pack_rows(4 * layer + 3 - half, 0, row_b, *groups_of(q, half))
+                send_stats(4 * layer + 3 - half)
 
         interleave(
             q + 1,
@@ -877,20 +921,6 @@
             chunk_total if layer else midway - 1,
             ready,
         )
-        for half in half_order:
-            def squares(index, half=half):
-                at_rows = tile_at(half * half_rows, index)
-                total = jnp.zeros((ROW_TILE, LANES), jnp.float32)
-                for s in range(strips):
-                    own = acc[0, at_rows, strip(s)].astype(jnp.bfloat16).astype(jnp.float32)
-                    total = total + own * own
-                row_a[at_rows, :] = total
-
-            loop(half_tiles, squares)
-        pack_rows(event + 2, 0, row_a)
-        send_stats(event + 2)
-        spread_rows(scale_ref, lax.rsqrt(total_stats(event + 2) / model + 1e-06), 0)
-
         def updated(at_rows, layer=layer):
             branch = acc[0, at_rows, :].astype(jnp.bfloat16).astype(jnp.float32)
             scale = jnp.concatenate([scale_ref[at_rows, :]] * strips, axis=1)
@@ -903,33 +933,32 @@
                 last[at_rows, :] = after
             return after.astype(jnp.float32)
 
-        if layer + 1 < layers:
-            for half in half_order:
+        for half in half_order:
+            scale = lax.rsqrt(total_stats(event + 3 - half) / model + 1e-06)
+            spread_rows(scale_ref, scale, 0, *groups_of(q + 1, half))
+            if layer + 1 < layers:
                 emit_u(layer + 1, half, updated)
                 send_own(q + 2, half)
-            pack_rows(event + 3, 0, row_a)
-            send_stats(event + 3)
-        else:
-            for half in half_order:
-                loop(half_tiles, lambda index, half=half: updated(tile_at(half * half_rows, index)))
+                if half == 0:
+                    pack_rows(event + 4, 0, row_a)
+                    send_stats(event + 4)
+            else:
+                tiles(q + 1, half, lambda start, tile: updated(pl.ds(start, tile)))
                 result_copy(half).start()
 
-    for way in range(2):
-        for chunk in range(2 * pieces):
-            for step in range(group_turns):
-                sub_copy(chunk, step, way).wait_send()
-        for chunk in range(2 * pieces, chunk_total):
-            for step in range(turns):
-                ring_copy(chunk, step, way).wait_send()
+    sent = 2 * ((group_turns - 1) * piece + piece // 2)
+    await_bytes(w_all.at[0, 0 : 2 * pieces * sent, :], sub_send.at[0])
+    for chunk in range(chunk_total - 2 * pieces):
+        await_bytes(
+            w_all.at[0, 0 : 2 * ((turns - 1) * piece + piece // 2), :], ring_send.at[chunk]
+        )
     for which in range(2):
         for half in range(HALVES):
             half_copy(which, half).wait_send()
     for q in range(2 * layers):
         drain(q)
-    for step in range(1, count):
-        for event in range(3 * layers):
-            stat_copy(event, step).wait_send()
-        param_copy(step).wait_send()
+    await_bytes(stat_in, stat_send.at[0])
+    await_bytes(params.at[0 : count - 1], par_send.at[0])
 
     @pl.when(has_next)
     def _():
@@ -976,21 +1005,22 @@
         dma((HALVES,)),
         pltpu.VMEM((layers, HALO_ROWS, width), jnp.bfloat16),
         pltpu.VMEM((layers, HALO_ROWS, width), jnp.bfloat16),
-        pltpu.VMEM((3 * layers, stat_rows, LANES), jnp.float32),
-        pltpu.VMEM((3 * layers, count - 1, stat_rows, LANES), jnp.float32),
+        pltpu.VMEM((4 * layers, stat_rows, LANES), jnp.float32),
+        pltpu.VMEM((4 * layers, count - 1, stat_rows, LANES), jnp.float32),
         pltpu.VMEM((count, param_rows, width), jnp.float32),
         pltpu.VMEM((count, rows, width), jnp.bfloat16),
         pltpu.VMEM((2, rows, width), jnp.bfloat16),
         pltpu.VMEM((2, rows, width), jnp.bfloat16),
     ]
-    scratch += [dma((2 * layers, chips, HALVES))] * 5
-    scratch += [dma((2, chunks, ring // 2))] * 2
-    scratch += [dma((2, 2 * pieces, max(1, ring // 4)))] * 2
-    scratch += [dma((chunks,))]
+    scratch += [dma((2 * layers,))] * 2 + [dma((2 * layers, chips, HALVES))]
+    scratch += [dma((2 * layers,)), dma((2 * layers, chips, HALVES))]
+    scratch += [dma((chunks - 2 * pieces,)), dma((chunks - 2 * pieces, ring // 2))]
+    scratch += [dma((1,)), dma((2, 2 * pieces, max(1, ring // 4)))]
+    scratch += [dma((3 * layers,))]
     scratch += [dma((chips, HALVES))] * 4
     scratch += [dma((2, HALVES))] * 2
-    scratch += [dma((3 * layers, count - 1))] * 2
-    scratch += [dma((count - 1,))] * 2
+    scratch += [dma((1,)), dma((4 * layers, count - 1))]
+    scratch += [dma((1,)), dma((count - 1,))]
     scratch += [dma((layers,))] * 2
     flops = 2 * rows * model_width(tokens, count) * width * 3 * layers
     return pl.pallas_call(

time: 216 us -> 209 us (0.968)
  Pallas kernels: 214 us -> 207 us
    pallas_call x1, Pallas kernels: 214 us -> 207 us  [shards(): pl.pallas_call(functools.partial(module_kernel, ring, count), out_shape=j...]
where the time goes in v2:
time: 209 us
  Pallas kernels  207 us (99%)
    pallas_call x1, Pallas kernels, shards(): pl.pallas_call(functools.partial(module_kernel, ring, count), out_shape=j...  207 us

profile of v2, /device:TPU:0, one launch (start us, length us, event | category | flops | bytes accessed | tf_op | source)
XLA Modules:
  0.0 209.2 jit_solution(10427050713689076743)
XLA Ops:
  0.0 207.3 %modules.1 = bf16[512,512]{1,0:T(8,128)(2,1)} custom-call(bf16[512,512]{1,0:T(8,128)(2,1)} %tok_hbm.1, f32[2,4096]{1,0:T(2,128)} %pre_hbm.1, bf16[2,1024,512]{2,1,0:T(8,128)(2,1)} %value_ref.1, bf16[2,1024,512]{2,1,0:T(8,128)(2,1)} %gate_ref.1, bf16[2,1024,512]{2,1,0:T(8,128)(2,1)} %wout_ref.1, f32[31,2,512]{2,1,0:T(2,128)} %bitcast.1, f32[2,512]{1,0:T(2,128)} %bias_hbm.1, ...), custom_call_target="tpu_custom_call" | custom-call | flops 12884901888 | bytes 25165824 | tf_op jit(solution)/shard_map/modules/pallas_call | solution.py:1026
  207.3 1.9 copy.12

commit v3 on v2

--- a/solution.py
+++ b/solution.py
@@ -60,7 +60,10 @@
     ngain_hbm,
     nbias_hbm,
     post_hbm,
-    out_ref,
+    last,
+    stream,
+    final,
+    gain_ref,
     tok_ref,
     pre_ref,
     taps_ref,
@@ -80,9 +83,6 @@
     row_b,
     scale_ref,
     shift_ref,
-    stream,
-    last,
-    last_sem,
     halo_out,
     halo_in,
     stat_out,
@@ -272,6 +272,19 @@
         size = 2 * piece if step < turns - 1 else piece
         await_bytes(w_all.at[0, 0:size, :], ring_recv.at[chunk - 2 * pieces, step])
 
+    def whole_turn(chunk):
+        owner = gray_of((at + ring - (2 * x_way - 1)) % ring, ring)
+        there = held(chunk, owner, 0, piece)
+        return remote(
+            there,
+            there,
+            ring_send.at[chunk - 2 * pieces],
+            ring_recv.at[chunk - 2 * pieces, turns - 1],
+            "sp",
+            ahead * x_way + behind * (1 - x_way),
+        )
+
+    second = 3 * pieces
     started = [3 * pieces]
 
     def start_until(last):
@@ -283,8 +296,11 @@
     def turn_chunk(chunk, most):
         for step in range(turns - 1):
             ring_arrived(chunk, step)
-            for way in range(2):
-                ring_copy(chunk, step + 1, way).start()
+            if ring == 4 and chunk == second:
+                whole_turn(chunk).start()
+            else:
+                for way in range(2):
+                    ring_copy(chunk, step + 1, way).start()
         if chunk < 5 * pieces - 1:
             most = min(most, 5 * pieces - 1)
         start_until(min(chunk + AHEAD, most))
@@ -451,7 +467,7 @@
             stat_out.at[event],
             stat_in.at[event, step - 1],
             stat_send.at[0],
-            stat_recv.at[event, step - 1],
+            stat_recv.at[event],
             "tp",
             lax.rem(me + step, count),
         )
@@ -469,8 +485,8 @@
 
     def total_stats(event):
         total = stat_out[event]
+        await_bytes(stat_in.at[event], stat_recv.at[event])
         for step in range(1, count):
-            stat_copy(event, step).wait_recv()
             total = total + stat_in[event, step - 1]
         return total
 
@@ -681,7 +697,7 @@
             params.at[me],
             params.at[me],
             par_send.at[0],
-            par_recv.at[step - 1],
+            par_recv.at[0],
             "tp",
             lax.rem(me + step, count),
         )
@@ -694,10 +710,6 @@
     send_stats(0)
     for step in range(1, count):
         param_copy(step).start()
-
-    def result_copy(half):
-        at_rows = rows_of(2 * layers - 1, half)
-        return pltpu.make_async_copy(last.at[at_rows, :], out_ref.at[at_rows, :], last_sem.at[half])
 
     def halo_copy(layer):
         return remote(
@@ -760,7 +772,6 @@
         send_own(2 * layer + 1, half)
 
     first_out = 2 * pieces
-    second = 3 * pieces
     midway = 5 * pieces + 1
     turns_of = (
         range(second - 1, second + pieces - 1),
@@ -859,11 +870,41 @@
                 start_until(midway + AHEAD - 1)
             emit_f(layer, half)
 
-    def squares(start, tile):
+    def merge_chunk(layer, chunk, first):
+        offset = (chunk % pieces) * piece
+
+        def body(index):
+            total = None
+            for each in range(-1, chips - 2):
+                chip = z if each < 0 else arrival(each)
+                for c in range(2):
+                    if c % blocks_held != offset // width:
+                        continue
+                    block = 2 * chip + c
+                    start = block * width + offset % width
+                    product = jnp.dot(
+                        mixed[block, :, offset % width : offset % width + piece],
+                        w_all[
+                            3 * layer + 2, pl.ds(pl.multiple_of(start, piece), piece), columns(index)
+                        ],
+                        preferred_element_type=jnp.float32,
+                    )
+                    total = product if total is None else total + product
+            if first:
+                acc[0, :, columns(index)] = total
+            else:
+                acc[0, :, columns(index)] += total
+
+        loop(width // column_tile, body)
+
+    def squares(layer, start, tile):
         at_rows = pl.ds(start, tile)
         total = jnp.zeros((tile, LANES), jnp.float32)
         for s in range(strips):
-            own = acc[0, at_rows, strip(s)].astype(jnp.bfloat16).astype(jnp.float32)
+            branch = acc[0, at_rows, strip(s)].astype(jnp.bfloat16)
+            if layer == layers - 1:
+                last[at_rows, strip(s)] = branch
+            own = branch.astype(jnp.float32)
             total = total + own * own
         row_b[at_rows, :] = total
 
@@ -884,8 +925,7 @@
             spread_rows(scale_ref, inverse, 0)
             spread_rows(shift_ref, centre * inverse, 0)
             if layer == 0:
-                for step in range(1, count):
-                    param_copy(step).wait_recv()
+                await_bytes(params.at[0 : count - 1], par_recv.at[0])
             for half in half_order:
                 side_wait(2 * layer + 1, z, half)
                 mix(layer, z, half)
@@ -903,14 +943,12 @@
             if index == chips - 2 and half == half_order[0]:
                 for chunk in range((3 * layer + 2) * pieces, (3 * layer + 3) * pieces):
                     finish_chunk(chunk)
-                for each in half_order:
-                    for done in range(-1, chips - 2):
-                        merge(layer, z if done < 0 else arrival(done), each, done < 0)
+                    merge_chunk(layer, chunk, chunk % pieces == 0)
             side_wait(q, arrival(index), half)
             mix(layer, arrival(index), half)
             if index == chips - 2:
                 merge(layer, arrival(index), half, False)
-                tiles(q, half, squares)
+                tiles(q, half, functools.partial(squares, layer))
                 pack_rows(4 * layer + 3 - half, 0, row_b, *groups_of(q, half))
                 send_stats(4 * layer + 3 - half)
 
@@ -927,25 +965,26 @@
             before = (tok_ref if layer == 0 else stream)[at_rows, :].astype(jnp.float32)
             after = before + branch * scale * post_ref[layer : layer + 1, :]
             after = after.astype(jnp.bfloat16)
+            stream[at_rows, :] = after
+            return after.astype(jnp.float32)
+
+        for half in half_order:
+            totals = total_stats(event + 3 - half)
             if layer + 1 < layers:
-                stream[at_rows, :] = after
-            else:
-                last[at_rows, :] = after
-            return after.astype(jnp.float32)
-
-        for half in half_order:
-            scale = lax.rsqrt(total_stats(event + 3 - half) / model + 1e-06)
-            spread_rows(scale_ref, scale, 0, *groups_of(q + 1, half))
-            if layer + 1 < layers:
+                scale = lax.rsqrt(totals / model + 1e-06)
+                spread_rows(scale_ref, scale, 0, *groups_of(q + 1, half))
                 emit_u(layer + 1, half, updated)
                 send_own(q + 2, half)
                 if half == 0:
                     pack_rows(event + 4, 0, row_a)
                     send_stats(event + 4)
             else:
-                tiles(q + 1, half, lambda start, tile: updated(pl.ds(start, tile)))
-                result_copy(half).start()
-
+                first, end = groups_of(q + 1, half)
+                final[first:end, :] = totals[first:end, :]
+
+    gain_ref[...] = post_ref[layers - 1 : layers, :]
+    if layers == 1:
+        stream[...] = tok_ref[...]
     sent = 2 * ((group_turns - 1) * piece + piece // 2)
     await_bytes(w_all.at[0, 0 : 2 * pieces * sent, :], sub_send.at[0])
     for chunk in range(chunk_total - 2 * pieces):
@@ -964,9 +1003,6 @@
     def _():
         for layer in range(layers):
             halo_copy(layer).wait_send()
-
-    for half in half_order:
-        result_copy(half).wait()
 
 
 def shards(
@@ -1000,9 +1036,6 @@
         pltpu.VMEM((rows, LANES), jnp.float32),
         pltpu.VMEM((rows, LANES), jnp.float32),
         pltpu.VMEM((rows, LANES), jnp.float32),
-        pltpu.VMEM((rows, width), jnp.bfloat16),
-        pltpu.VMEM((rows, width), jnp.bfloat16),
-        dma((HALVES,)),
         pltpu.VMEM((layers, HALO_ROWS, width), jnp.bfloat16),
         pltpu.VMEM((layers, HALO_ROWS, width), jnp.bfloat16),
         pltpu.VMEM((4 * layers, stat_rows, LANES), jnp.float32),
@@ -1019,18 +1052,23 @@
     scratch += [dma((3 * layers,))]
     scratch += [dma((chips, HALVES))] * 4
     scratch += [dma((2, HALVES))] * 2
-    scratch += [dma((1,)), dma((4 * layers, count - 1))]
-    scratch += [dma((1,)), dma((count - 1,))]
+    scratch += [dma((1,)), dma((4 * layers,))]
+    scratch += [dma((1,)), dma((1,))]
     scratch += [dma((layers,))] * 2
     flops = 2 * rows * model_width(tokens, count) * width * 3 * layers
-    return pl.pallas_call(
+    branch, before, totals, gain = pl.pallas_call(
         functools.partial(module_kernel, ring, count),
-        out_shape=jax.ShapeDtypeStruct(tokens.shape, tokens.dtype),
+        out_shape=[
+            pltpu.VMEM(tokens.shape, tokens.dtype),
+            pltpu.VMEM(tokens.shape, tokens.dtype),
+            pltpu.VMEM((stat_rows, LANES), jnp.float32),
+            pltpu.VMEM((1, width), jnp.float32),
+        ],
         in_specs=[hbm] * 10,
-        out_specs=hbm,
+        out_specs=[pl.BlockSpec(memory_space=pltpu.VMEM)] * 4,
         scratch_shapes=scratch,
         compiler_params=pltpu.CompilerParams(
-            collective_id=0, has_side_effects=True, vmem_limit_bytes=63 * 2**20
+            collective_id=0, has_side_effects=True, vmem_limit_bytes=60 * 2**20
         ),
         cost_estimate=pl.CostEstimate(flops=flops, bytes_accessed=flops // 512, transcendentals=0),
         name="modules",
@@ -1046,6 +1084,10 @@
         norm_bias,
         post_gain,
     )
+    total = totals[: rows // LANES].reshape(rows)
+    rescale = lax.rsqrt(total / model_width(tokens, count) + 1e-06)[:, None]
+    after = before.astype(jnp.float32) + branch.astype(jnp.float32) * rescale * gain
+    return after.astype(jnp.bfloat16)
 
 
 def model_width(tokens, count):

time: 209 us -> 203 us (0.971)
  Pallas kernels: 207 us -> 202 us
    pallas_call x1, Pallas kernels: 207 us -> 202 us  [shards(): pl.pallas_call(functools.partial(module_kernel, ring, count), out_shape=[...]
where the time goes in v3:
time: 203 us
  Pallas kernels  202 us (100%)
    pallas_call x1, Pallas kernels, shards(): pl.pallas_call(functools.partial(module_kernel, ring, count), out_shape=[...  202 us

profile of v3, /device:TPU:0, one launch (start us, length us, event | category | flops | bytes accessed | tf_op | source)
XLA Modules:
  0.0 203.0 jit_solution(446700676063424855)
XLA Ops:
  0.0 201.9 %modules.1 = (bf16[512,512]{1,0:T(8,128)(2,1)S(1)}, bf16[512,512]{1,0:T(8,128)(2,1)S(1)}, f32[8,128]{1,0:T(8,128)S(1)}, f32[1,512]{1,0:T(1,128)S(1)}) custom-call(bf16[512,512]{1,0:T(8,128)(2,1)} %tok_hbm.1, f32[2,4096]{1,0:T(2,128)} %pre_hbm.1, bf16[2,1024,512]{2,1,0:T(8,128)(2,1)} %value_ref.1, bf16[2,1024,512]{2,1,0:T(8,128)(2,1)} %gate_ref.1, ...), custom_call_target="tpu_custom_call" | custom-call | flops 12884901888 | bytes 25165824 | tf_op jit(solution)/shard_map/modules/pallas_call | solution.py:1059
  201.9 1.1 add_convert_fusion
  (1 shorter events, 0.0 us)

commit v4 on v3

--- a/solution.py
+++ b/solution.py
@@ -201,11 +201,6 @@
     for load in loads:
         load.start()
 
-    pl.semaphore_wait(
-        barrier,
-        count + (3 if group > 2 else 1) + has_next.astype(jnp.int32) + has_prev.astype(jnp.int32)
-    )
-
     sources = (value_ref, gate_ref, wout_ref)
     chunk_total = 3 * layers * pieces
 
@@ -272,16 +267,17 @@
         size = 2 * piece if step < turns - 1 else piece
         await_bytes(w_all.at[0, 0:size, :], ring_recv.at[chunk - 2 * pieces, step])
 
-    def whole_turn(chunk):
-        owner = gray_of((at + ring - (2 * x_way - 1)) % ring, ring)
-        there = held(chunk, owner, 0, piece)
+    def uneven_turn(chunk, way, first, size):
+        owner = gray_of((at + ring - (1 - 2 * way)) % ring, ring)
+        start = owner * depth + (chunk % pieces) * piece + first
+        there = w_all.at[chunk // pieces, pl.ds(pl.multiple_of(start, piece // 4), size), :]
         return remote(
             there,
             there,
             ring_send.at[chunk - 2 * pieces],
             ring_recv.at[chunk - 2 * pieces, turns - 1],
             "sp",
-            ahead * x_way + behind * (1 - x_way),
+            ahead * (1 - way) + behind * way,
         )
 
     second = 3 * pieces
@@ -297,7 +293,9 @@
         for step in range(turns - 1):
             ring_arrived(chunk, step)
             if ring == 4 and chunk == second:
-                whole_turn(chunk).start()
+                most_rows = 3 * (piece // 4)
+                uneven_turn(chunk, 1 - x_way, 0, most_rows).start()
+                uneven_turn(chunk, x_way, most_rows, piece - most_rows).start()
             else:
                 for way in range(2):
                     ring_copy(chunk, step + 1, way).start()
@@ -675,21 +673,27 @@
 
         loop(width // column_tile, body)
 
+    for load in loads[:4]:
+        load.wait()
+
+    def from_tokens(at_rows):
+        return tok_ref[at_rows, :].astype(jnp.float32)
+
+    for half in half_order:
+        emit_u(0, half, from_tokens)
+    for layer in range(layers):
+        params[me, 2 * layer : 2 * layer + 1, :] = ngain_ref[layer : layer + 1, :]
+        params[me, 2 * layer + 1 : 2 * layer + 2, :] = nbias_ref[layer : layer + 1, :]
+    pack_rows(0, 0, row_a)
+    pl.semaphore_wait(
+        barrier,
+        count + (3 if group > 2 else 1) + has_next.astype(jnp.int32) + has_prev.astype(jnp.int32)
+    )
+
     for chunk in range(2 * pieces):
         for way in range(2):
             sub_copy(chunk, 0, way).start()
-    for load in loads[:4]:
-        load.wait()
-
-    def from_tokens(at_rows):
-        return tok_ref[at_rows, :].astype(jnp.float32)
-
     for half in half_order:
-        emit_u(0, half, from_tokens)
-        if half == half_order[0]:
-            for layer in range(layers):
-                params[me, 2 * layer : 2 * layer + 1, :] = ngain_ref[layer : layer + 1, :]
-                params[me, 2 * layer + 1 : 2 * layer + 2, :] = nbias_ref[layer : layer + 1, :]
         send_own(0, half)
 
     def param_copy(step):
@@ -706,7 +710,6 @@
         ring_copy(chunk, 0, 1 - x_way).start()
     for projection in range(3 * layers):
         own_copy(projection).start()
-    pack_rows(0, 0, row_a)
     send_stats(0)
     for step in range(1, count):
         param_copy(step).start()
@@ -908,6 +911,26 @@
             total = total + own * own
         row_b[at_rows, :] = total
 
+    def settle():
+        sent = 2 * ((group_turns - 1) * piece + piece // 2)
+        await_bytes(w_all.at[0, 0 : 2 * pieces * sent, :], sub_send.at[0])
+        for chunk in range(chunk_total - 2 * pieces):
+            await_bytes(
+                w_all.at[0, 0 : 2 * ((turns - 1) * piece + piece // 2), :], ring_send.at[chunk]
+            )
+        for which in range(2):
+            for half in range(HALVES):
+                half_copy(which, half).wait_send()
+        for q in range(2 * layers):
+            drain(q)
+        await_bytes(stat_in, stat_send.at[0])
+        await_bytes(params.at[0 : count - 1], par_send.at[0])
+
+        @pl.when(has_next)
+        def _():
+            for layer in range(layers):
+                halo_copy(layer).wait_send()
+
     for layer in range(layers):
         q = 2 * layer
         event = 4 * layer
@@ -968,6 +991,8 @@
             stream[at_rows, :] = after
             return after.astype(jnp.float32)
 
+        if layer == layers - 1:
+            settle()
         for half in half_order:
             totals = total_stats(event + 3 - half)
             if layer + 1 < layers:
@@ -985,24 +1010,6 @@
     gain_ref[...] = post_ref[layers - 1 : layers, :]
     if layers == 1:
         stream[...] = tok_ref[...]
-    sent = 2 * ((group_turns - 1) * piece + piece // 2)
-    await_bytes(w_all.at[0, 0 : 2 * pieces * sent, :], sub_send.at[0])
-    for chunk in range(chunk_total - 2 * pieces):
-        await_bytes(
-            w_all.at[0, 0 : 2 * ((turns - 1) * piece + piece // 2), :], ring_send.at[chunk]
-        )
-    for which in range(2):
-        for half in range(HALVES):
-            half_copy(which, half).wait_send()
-    for q in range(2 * layers):
-        drain(q)
-    await_bytes(stat_in, stat_send.at[0])
-    await_bytes(params.at[0 : count - 1], par_send.at[0])
-
-    @pl.when(has_next)
-    def _():
-        for layer in range(layers):
-            halo_copy(layer).wait_send()
 
 
 def shards(

time: 203 us -> 203 us (level)
  no operation moved by 1% of the time
where the time goes in v4:
time: 203 us
  Pallas kernels  201 us (99%)
    pallas_call x1, Pallas kernels, shards(): pl.pallas_call(functools.partial(module_kernel, ring, count), out_shape=[...  201 us

profile of v4, /device:TPU:0, one launch (start us, length us, event | category | flops | bytes accessed | tf_op | source)
XLA Modules:
  0.0 202.5 jit_solution(16089261169322241853)
XLA Ops:
  0.0 201.5 %modules.1 = (bf16[512,512]{1,0:T(8,128)(2,1)S(1)}, bf16[512,512]{1,0:T(8,128)(2,1)S(1)}, f32[8,128]{1,0:T(8,128)S(1)}, f32[1,512]{1,0:T(1,128)S(1)}) custom-call(bf16[512,512]{1,0:T(8,128)(2,1)} %tok_hbm.1, f32[2,4096]{1,0:T(2,128)} %pre_hbm.1, bf16[2,1024,512]{2,1,0:T(8,128)(2,1)} %value_ref.1, bf16[2,1024,512]{2,1,0:T(8,128)(2,1)} %gate_ref.1, ...), custom_call_target="tpu_custom_call" | custom-call | flops 12884901888 | bytes 25165824 | tf_op jit(solution)/shard_map/modules/pallas_call | solution.py:1066
  201.5 1.1 add_convert_fusion
  (1 shorter events, 0.0 us)
